TPU v7x, 32 devices: a whole 2x2x4 slice. The times are simulated.
32 devices in a mesh: sp: 16 (over z, y, x), tp: 2 (over core).
Axes of the slice: x: 2, y: 2, z: 4, core: 2. Of those that a mesh axis runs over, the one named last changes fastest.
Arguments:
- queries: bfloat16 [2048, 768], P('sp', 'tp'), may hold values from -6 to 6
- latents: bfloat16 [2048, 512], P('sp'), may hold values from -6 to 6
- rot_key: bfloat16 [2048, 32], P('sp'), may hold values from -6 to 6
- kv_weight: bfloat16 [512, 1024], P(None, 'tp'), may hold values from -0.25 to 0.25
- log_sums: float32 [2048, 8], P('sp', 'tp'), may hold values from 4 to 14, as said below
- outputs: bfloat16 [2048, 512], P('sp', 'tp'), may hold values from -4 to 4
- out_grad: bfloat16 [2048, 512], P('sp', 'tp'), may hold values from -96 to 96
Outputs:
- query_grad: bfloat16 [2048, 768], P('sp', 'tp')
- key_grad: bfloat16 [2048, 512], P('sp', 'tp')
- value_grad: bfloat16 [2048, 512], P('sp', 'tp')
- rot_grad: float32 [2048, 32], P('sp')
- weight_grad: float32 [512, 1024], P('sp', 'tp')
Inputs may be any that keep to these rules, and one draw needn't show every extreme that they name: `log_sums`: each value lies within one half of log(2048) + 0.5.
All inputs are finite; a program needn't handle non-finite values.
Results may differ from a plain program's by a relative error of at most 0.004.
The roundings to bfloat16 on the way count: a program that leaves them out, or rounds other values in their place, can miss the bound.
Values may be sent and summed in bfloat16 or wider, within the bound.
A program may use at most 64 MiB of HBM per device.

v0:
```python
import functools
import math

import jax
import jax.numpy as jnp
from jax import lax
from jax.experimental import pallas as pl
from jax.experimental.pallas import tpu as pltpu
from jax.sharding import PartitionSpec as P

NOPE = 64
ROPE = 32
VDIM = 64
HEAD = NOPE + ROPE
VMEM_BYTES = 67043328
SPARE = 8192
MESH = pl.DeviceIdType.MESH
F32 = jnp.float32
BF16 = jnp.bfloat16


def dot(x, y, dims):
    return lax.dot_general(x, y, (dims, ((), ())), preferred_element_type=F32)


def three_terms(x):
    hi = x.astype(BF16)
    rest = x - hi.astype(F32)
    mid = rest.astype(BF16)
    low = (rest - mid.astype(F32)).astype(BF16)
    return hi, mid, low


def repeat(start, stop, body):
    if stop - start <= 4:
        for i in range(start, stop):
            body(i)
    else:
        def step(i, carry):
            body(i)
            return carry

        lax.fori_loop(start, stop, step, 0)


def kernel(
    S, TP, H,
    q_in, lat_in, rot_in, w_in, log_in, out_in, go_in,
    qg_ref, kg_ref, vg_ref, rg_ref, wg_ref,
    q_ref, lat_ref, rot_ref, w_ref, log_ref, out_ref, go_ref, loads, ps, pk, wq, kb, lb, ka_ref, va_ref, kat_ref, dk_acc, dv_acc, dq_own, dqs, dqr,
    kvo, kvr, ro, rr, rt, wgs, wgr, wh, wo, qo, qr,
    s1q, r1q, s1k, r1k, s1l, r1l, s2, r2, s3, r3, s4k, r4k, s4r, r4r, s4q, r4q, s5, r5, s6, r6, s7, r7, s8, r8,
):
    G = S // H
    T = q_ref.shape[0]
    half = T // 2
    me = lax.axis_index("sp")
    tpi = lax.axis_index("tp")
    a, b = me // G, lax.rem(me, G)
    scale = HEAD ** (-0.5)

    barrier = pltpu.get_barrier_semaphore()

    def greet(i):
        pl.semaphore_signal(barrier, inc=1, device_id={"sp": lax.rem(me + i, S)}, device_id_type=MESH)

    def greet_tp(i):
        pl.semaphore_signal(barrier, inc=1, device_id={"tp": lax.rem(tpi + i, TP)}, device_id_type=MESH)

    pairs = (
        (q_in, q_ref), (go_in, go_ref), (out_in, out_ref), (log_in, log_ref),
        (lat_in, lat_ref), (w_in, w_ref), (rot_in, rot_ref),
    )
    fetch = [pltpu.make_async_copy(x, y, loads.at[i]) for i, (x, y) in enumerate(pairs)]
    for f in fetch:
        f.start()
    repeat(1, S, greet)
    repeat(1, TP, greet_tp)

    def copy(src, dst, ssem, rsem, sp):
        return pltpu.make_async_remote_copy(
            src_ref=src, dst_ref=dst, send_sem=ssem, recv_sem=rsem,
            device_id={"sp": sp}, device_id_type=MESH,
        )

    for f in fetch[:4]:
        f.wait()
    logs_t = log_ref[...] * math.sqrt(HEAD)
    prod = out_ref[...].astype(F32) * go_ref[...].astype(F32)
    pad = jnp.zeros((T, ROPE - 6), BF16)
    for j in range(H):
        delta = jnp.sum(prod[:, VDIM * j : VDIM * (j + 1)], axis=1, keepdims=True)
        logs = jnp.broadcast_to(logs_t[j : j + 1], (8, T)).T[:, :1]
        terms = three_terms(logs) + three_terms(delta)
        ps[j, :T, :] = jnp.concatenate([q_ref[:, HEAD * j : HEAD * (j + 1)], *terms, pad], axis=1)
        g = go_ref[:, VDIM * j : VDIM * (j + 1)]
        ps[j, T:, :] = jnp.concatenate([g[:half], g[half:]], axis=1)
    wq[b, a] = ps[a]
    pl.semaphore_wait(barrier, S - 1 + TP - 1)

    firsts, lats = [], []
    for d in range(1, H):
        to = lax.rem(a + d, H)
        cq = copy(ps.at[to], wq.at[b, a], s1q.at[d - 1], r1q.at[d - 1], to * G + b)
        ck = copy(pk.at[to], kb.at[a], s1k.at[d - 1], r1k.at[d - 1], to * G + b)
        cq.start()
        firsts.append((cq, ck))

    def relay(d, e):
        src = wq.at[b, lax.rem(a - d + H, H)]
        return copy(src, src, s2.at[e - 1, d], r2.at[e - 1, d], a * G + lax.rem(b + e, G))

    def relay_all(d):
        repeat(1, G, lambda e: relay(d, e).start())

    relay_all(0)
    for f in fetch[4:]:
        f.wait()
    joined = dot(lat_ref[...], w_ref[...], ((1,), (0,))).astype(BF16)
    for j in range(H):
        pk[j, :T, :] = joined[:, 128 * j : 128 * (j + 1)]
        pk[j, T:, :] = rot_ref[...]
    kb[a] = pk[a]
    for d in range(1, H):
        firsts[d - 1][1].start()
    lb[a] = lat_ref[...].reshape(lb.shape[1:])
    slab = T // TP
    mine = lat_ref.at[pl.ds(pl.multiple_of(tpi * slab, slab), slab)]
    for d in range(1, H):
        to = lax.rem(a + d, H)
        cl = copy(mine, lb.at[a, tpi], s1l.at[d - 1], r1l.at[d - 1], to * G + b)
        cl.start()
        lats.append(cl)
    for d in range(1, H):
        firsts[d - 1][0].wait_recv()
        relay_all(d)
    for d in range(1, H):
        firsts[d - 1][1].wait_recv()

    lane = lax.broadcasted_iota(jnp.int32, (T, ROPE), 1)
    log_ones = jnp.where(lane < 3, -1.0, 0.0).astype(BF16)
    delta_ones = jnp.where((lane >= 3) & (lane < 6), -1.0, 0.0).astype(BF16)
    for j in range(H):
        kv = kb[j, :T, :]
        r = kb[j, T:, :].astype(F32).T.astype(BF16)
        key = jnp.concatenate([kv[:, :NOPE], r, log_ones], axis=1)
        ka_ref[T * j : T * (j + 1), :] = key
        va_ref[T * j : T * (j + 1), :128] = jnp.concatenate([jnp.zeros((T, HEAD), BF16), delta_ones], axis=1)
        va_ref[T * j : T * (j + 1), 128:] = jnp.concatenate([kv[:, NOPE:], jnp.zeros((T, 64), BF16)], axis=1)
        kat_ref[:, T * j : T * (j + 1)] = key.astype(F32).T.astype(BF16)[:HEAD]
    dk_acc[...] = jnp.zeros_like(dk_acc)
    dv_acc[...] = jnp.zeros_like(dv_acc)

    def block(e, keep):
        col = lax.rem(b - e + G, G)
        query = wq[col, :, :T, :].reshape(H * T, 128)
        gp = wq[col, :, T:, :]
        g = jnp.concatenate([gp[:, :, :VDIM], gp[:, :, VDIM:]], axis=1).reshape(H * T, VDIM)
        g = jnp.concatenate([g, jnp.zeros_like(g)], axis=1)
        s = dot(ka_ref[...], query, ((1,), (1,)))
        dp = dot(va_ref[...], jnp.concatenate([query, g], axis=1), ((1,), (1,)))
        p = jnp.exp(s * scale)
        ds = (p * dp).astype(BF16)
        keep(dot(kat_ref[...], ds, ((1,), (0,))) * scale)
        dv_acc[...] += dot(p.astype(BF16), g, ((1,), (0,)))
        dk_acc[...] += dot(ds, query, ((1,), (0,)))

    def part(e):
        return copy(dqs.at[e - 1], dqr.at[e - 1], s3.at[e - 1], r3.at[e - 1], a * G + lax.rem(b - e + G, G))

    def keep_own(x):
        dq_own[...] = x

    block(0, keep_own)

    def other(e):
        for d in range(H):
            relay(d, e).wait_recv()

        def send(x):
            dqs[e - 1] = x
            part(e).start()

        block(e, send)

    def hand_on(d, i):
        piece = lb.at[lax.rem(a - d + H, H), tpi]
        return pltpu.make_async_remote_copy(
            src_ref=piece, dst_ref=piece, send_sem=s8.at[d - 1, i - 1], recv_sem=r8.at[d - 1, i - 1],
            device_id={"tp": lax.rem(tpi + i, TP)}, device_id_type=MESH,
        )

    repeat(1, min(3, G), other)
    for d in range(1, H):
        lats[d - 1].wait_recv()
        repeat(1, TP, lambda i: hand_on(d, i).start())
    repeat(min(3, G), G, other)

    dk = dk_acc[...] * scale
    kv = jnp.concatenate([dk[:, :NOPE], dv_acc[:, :VDIM]], axis=1).astype(BF16)
    rot_t = dk.T[NOPE:HEAD]
    for j in range(H):
        kvo[j] = kv[T * j : T * (j + 1)]
        ro[j] = rot_t[:, T * j : T * (j + 1)]
    kvr[a] = kvo[a]
    rr[a] = ro[a]
    backs = []
    for d in range(1, H):
        to = lax.rem(a + d, H)
        ck = copy(kvo.at[to], kvr.at[a], s4k.at[d - 1], r4k.at[d - 1], to * G + b)
        cr = copy(ro.at[to], rr.at[a], s4r.at[d - 1], r4r.at[d - 1], to * G + b)
        cr.start()
        ck.start()
        backs += [ck, cr]

    for d in range(1, H):
        repeat(1, TP, lambda i: hand_on(d, i).wait_recv())
    lat = lb[...].reshape(H * T, lb.shape[3])
    total = dot(lat, kv, ((0,), (0,)))
    rows = wgs.shape[2]
    for i in range(G):
        for j in range(H):
            wgs[i, j] = total[(j * G + i) * rows : (j * G + i + 1) * rows]
    wgr[b] = wgs[b]

    def share(e):
        to = lax.rem(b + e, G)
        return copy(wgs.at[to], wgr.at[b], s5.at[e - 1], r5.at[e - 1], a * G + to)

    repeat(1, G, lambda e: share(e).start())

    def take(e):
        part(e).wait_recv()
        dq_own[...] += dqr[e - 1]

    repeat(1, G, take)
    dq = jnp.concatenate([dq_own[...], jnp.zeros((128 - HEAD, H * T), F32)], axis=0).T.astype(BF16)
    for j in range(H):
        qo[j] = dq[T * j : T * (j + 1)]
    qr[a] = qo[a]
    for d in range(1, H):
        to = lax.rem(a + d, H)
        cq = copy(qo.at[to], qr.at[a], s4q.at[d - 1], r4q.at[d - 1], to * G + b)
        cq.start()
        backs.append(cq)

    repeat(1, G, lambda e: share(e).wait_recv())
    wh[...] = functools.reduce(lambda x, y: x + y, [wgr[i] for i in range(G)])
    wo[a] = wh[a]
    lasts = []
    for d in range(1, H):
        to = lax.rem(a + d, H)
        c = copy(wh.at[to], wo.at[a], s7.at[d - 1], r7.at[d - 1], to * G + b)
        c.start()
        lasts.append(c)
    for d in range(1, H):
        backs[2 * (d - 1) + 1].wait_recv()
    rt[tpi] = functools.reduce(lambda x, y: x + y, [rr[j] for j in range(H)])

    def swap(i):
        return pltpu.make_async_remote_copy(
            src_ref=rt.at[tpi], dst_ref=rt.at[tpi], send_sem=s6.at[i - 1], recv_sem=r6.at[i - 1],
            device_id={"tp": lax.rem(tpi + i, TP)}, device_id_type=MESH,
        )

    repeat(1, TP, lambda i: swap(i).start())
    for d in range(1, H):
        backs[2 * (d - 1)].wait_recv()
    for j in range(H):
        kg_ref[:, NOPE * j : NOPE * (j + 1)] = kvr[j, :, :NOPE]
        vg_ref[:, VDIM * j : VDIM * (j + 1)] = kvr[j, :, NOPE:]
    repeat(1, TP, lambda i: swap(i).wait_recv())
    rot_sum = functools.reduce(lambda x, y: x + y, [rt[i] for i in range(TP)])
    rg_ref[...] = rot_sum
    for d in range(1, H):
        backs[2 * (H - 1) + d - 1].wait_recv()
    for j in range(H):
        qg_ref[:, HEAD * j : HEAD * (j + 1)] = qr[j, :, :HEAD]

    for c in lasts:
        c.wait_recv()
    for j in range(H):
        wg_ref[:, 128 * j : 128 * (j + 1)] = wo[j]

    for cq, ck in firsts:
        cq.wait_send()
        ck.wait_send()
    for c in lats + backs + lasts:
        c.wait_send()
    for d in range(H):
        repeat(1, G, lambda e: relay(d, e).wait_send())
    repeat(1, G, lambda e: part(e).wait_send())
    repeat(1, G, lambda e: share(e).wait_send())
    repeat(1, TP, lambda i: swap(i).wait_send())
    for d in range(1, H):
        repeat(1, TP, lambda i: hand_on(d, i).wait_send())


def put_out(*refs):
    copies = [pltpu.make_async_copy(refs[i], refs[5 + i], refs[10].at[i]) for i in range(5)]
    for c in copies:
        c.start()
    for c in copies:
        c.wait()


def per_device(S, TP, queries, latents, rot_key, kv_weight, log_sums, outputs, out_grad):
    T, rank = latents.shape
    H = log_sums.shape[1]
    G = S // H
    rows = rank // S
    wide = H * T
    dma = lambda *n: pltpu.SemaphoreType.DMA(tuple(max(k, 1) for k in n))
    pairs = lambda *n: [dma(*n), dma(*n)]
    vm = pltpu.VMEM
    g1 = max(G - 1, 1)
    arrays = (queries, latents, rot_key.T, kv_weight, log_sums.T, outputs, out_grad)
    scratch = [
        *[vm(x.shape, x.dtype) for x in arrays], dma(len(arrays)),
        vm((H, T + T // 2, 128), BF16), vm((H, T + ROPE, 128), BF16),
        vm((G, H, T + T // 2, 128), BF16), vm((H, T + ROPE, 128), BF16), vm((H, TP, T // TP, rank), BF16),
        vm((wide, 128), BF16), vm((wide, 256), BF16), vm((HEAD, wide), BF16),
        vm((wide, 128), F32), vm((wide, 128), F32), vm((HEAD, wide), F32),
        vm((g1, HEAD, wide), F32), vm((g1, HEAD, wide), F32),
        vm((H, T, 128), BF16), vm((H, T, 128), BF16), vm((H, ROPE, T), F32), vm((H, ROPE, T), F32),
        vm((TP, ROPE, T), F32), *[vm((G, H, rows, 128), F32)] * 2, *[vm((H, rows, 128), F32)] * 2,
        vm((H, T, 128), BF16), vm((H, T, 128), BF16),
        *pairs(H - 1), *pairs(H - 1), *pairs(H - 1), *pairs(G - 1, H), *pairs(G - 1),
        *pairs(H - 1), *pairs(H - 1), *pairs(H - 1), *pairs(G - 1), *pairs(TP - 1), *pairs(H - 1), *pairs(H - 1, TP - 1),
    ]
    shapes = [
        ((T, H * HEAD), BF16), ((T, H * NOPE), BF16), ((T, H * VDIM), BF16),
        ((ROPE, T), F32), ((rows, H * 128), F32),
    ]
    held = sum(x[0] * -(-x[1] // 128) * 128 * jnp.dtype(t).itemsize for x, t in shapes)
    results = pl.pallas_call(
        functools.partial(kernel, S, TP, H),
        out_shape=[pltpu.VMEM(*x) for x in shapes],
        in_specs=[pl.BlockSpec(memory_space=pltpu.HBM)] * 7,
        out_specs=[pl.BlockSpec(memory_space=vm)] * 5,
        scratch_shapes=scratch,
        compiler_params=pltpu.CompilerParams(
            collective_id=0, has_side_effects=True, vmem_limit_bytes=VMEM_BYTES - held - SPARE
        ),
    )(*arrays)
    query_grad, key_grad, value_grad, rot_grad, weight_grad = pl.pallas_call(
        put_out,
        out_shape=[jax.ShapeDtypeStruct(*x) for x in shapes],
        in_specs=[pl.BlockSpec(memory_space=vm)] * 5,
        out_specs=[pl.BlockSpec(memory_space=pltpu.HBM)] * 5,
        scratch_shapes=[dma(5)],
        compiler_params=pltpu.CompilerParams(vmem_limit_bytes=1 << 20),
    )(*results)
    return query_grad, key_grad, value_grad, rot_grad.T, weight_grad


def solution(mesh):
    placed = (
        P("sp", "tp"), P("sp", None), P("sp", None), P(None, "tp"),
        P("sp", "tp"), P("sp", "tp"), P("sp", "tp"),
    )
    return jax.shard_map(
        functools.partial(per_device, mesh.shape["sp"], mesh.shape["tp"]),
        mesh=mesh,
        in_specs=placed,
        out_specs=(P("sp", "tp"), P("sp", "tp"), P("sp", "tp"), P("sp", None), P("sp", "tp")),
        check_vma=False,
    )
```

profile of v0, /device:TPU:0, one launch (start us, length us, event | category | flops | bytes accessed | tf_op | source)
XLA Modules:
  0.0 38.6 jit_solution(5787247381838307675)
XLA Ops:
  0.6 37.2 %shard_map.110 = (bf16[128,384]{1,0:T(8,128)(2,1)S(1)}, bf16[128,256]{1,0:T(8,128)(2,1)S(1)}, bf16[128,256]{1,0:T(8,128)(2,1)S(1)}, f32[32,128]{1,0:T(8,128)S(1)}, f32[32,512]{1,0:T(8,128)S(1)}) custom-call(bf16[128,384]{1,0:T(8,128)(2,1)} %q_in.1, bf16[128,512]{1,0:T(8,128)(2,1)} %lat_in.1, bf16[32,128]{1,0:T(8,128)(2,1)} %bitcast.3, ...), custom_call_target="tpu_custom_call" | custom-call | tf_op jit(solution)/shard_map/pallas_call | solution.py:336
  37.9 0.8 %shard_map.111 = (bf16[128,384]{1,0:T(8,128)(2,1)}, bf16[128,256]{1,0:T(8,128)(2,1)}, bf16[128,256]{1,0:T(8,128)(2,1)}, f32[32,128]{1,0:T(8,128)}, f32[32,512]{1,0:T(8,128)}) custom-call(bf16[128,384]{1,0:T(8,128)(2,1)S(1)} %get-tuple-element.15.refs_0_, bf16[128,256]{1,0:T(8,128)(2,1)S(1)} %get-tuple-element.16.refs_1_, ...), custom_call_target="tpu_custom_call" | custom-call | tf_op jit(solution)/shard_map/pallas_call | solution.py:346
where the time goes:
time: 38.8 us; the launch traced here: 38.6 us
  Pallas kernels  38 us (98%)
  between operations  0.64 us (2%)
    pallas_call x1, Pallas kernels, per_device(): pl.pallas_call(functools.partial(kernel, S, TP, H), out_shape=[pltpu.VMEM...  37.2 us

commit v1 on v0

v1 whole, which is shorter than its diff:
```python
import functools
import math

import jax
import jax.numpy as jnp
from jax import lax
from jax.experimental import pallas as pl
from jax.experimental.pallas import tpu as pltpu
from jax.sharding import PartitionSpec as P

NOPE = 64
ROPE = 32
VDIM = 64
HEAD = NOPE + ROPE
LANES = 128
STATS = 8
VMEM_BYTES = 67043328
SPARE = 8192
MESH = pl.DeviceIdType.MESH
F32 = jnp.float32
BF16 = jnp.bfloat16
KV_PART = BF16
DQ_PART = F32
WG_PART = BF16


def dot(x, y, dims):
    return lax.dot_general(x, y, (dims, ((), ())), preferred_element_type=F32)


def three_terms(x):
    hi = x.astype(BF16)
    rest = x - hi.astype(F32)
    mid = rest.astype(BF16)
    low = (rest - mid.astype(F32)).astype(BF16)
    return hi, mid, low


def repeat(start, stop, body):
    if stop - start <= 4:
        for i in range(start, stop):
            body(i)
    else:
        def step(i, carry):
            body(i)
            return carry

        lax.fori_loop(start, stop, step, 0)


def add_all(terms):
    return functools.reduce(lambda x, y: x + y, terms)


def power_of_two(n):
    return n & (n - 1) == 0


def partner(n, i, d, sign):
    if not power_of_two(n):
        return lax.rem(i + sign * d + n, n)
    bit = 1
    result = i
    while bit <= d:
        if d & bit:
            result = result + bit * (1 - 2 * lax.rem(i // bit, 2))
        bit *= 2
    return result


def distances(n):
    if not power_of_two(n):
        return list(range(1, n))
    return list(range(n // 2, n)) + list(range(1, n // 2))


def kernel(
    S, TP, H, GY, GX,
    q_in, lat_in, rot_in, w_in, log_in, out_in, go_in,
    qg_ref, kg_ref, vg_ref, rg_ref, wg_ref,
    q_ref, lat_ref, rot_ref, w_ref, log_ref, out_ref, go_ref, loads,
    qs, pk, wq, kb, lb, rp, dqa, dqs, dqr, kvs, kvr, own_kv, own_rot,
    kvo, kvh, ro, rr, rt, wgs, wgr, dqo, dqh,
    s1q, r1q, s1k, r1k, s1l, r1l, s2q, r2q, s2k, r2k, s3q, r3q, s3k, r3k,
    s4q, r4q, s4k, r4k, s4r, r4r, s5, r5, s6, r6, s8, r8,
):
    G = GY * GX
    T = q_ref.shape[0]
    me = lax.axis_index("sp")
    tpi = lax.axis_index("tp")
    a, b = me // G, lax.rem(me, G)
    y, x = b // GX, lax.rem(b, GX)
    scale = HEAD ** (-0.5)
    log2e = math.log2(math.e)
    far = distances(H)
    quarter = T * ROPE // LANES

    barrier = pltpu.get_barrier_semaphore()

    def greet(to):
        pl.semaphore_signal(barrier, inc=1, device_id={"sp": to}, device_id_type=MESH)

    def greet_tp(i):
        pl.semaphore_signal(barrier, inc=1, device_id={"tp": lax.rem(tpi + i, TP)}, device_id_type=MESH)

    def at_z(z):
        return z * G + b

    def at_y(e):
        return a * G + lax.rem(y + e, GY) * GX + x

    def at_x(e):
        return a * G + y * GX + lax.rem(x + e, GX)

    pairs = (
        (q_in, q_ref), (go_in, go_ref), (out_in, out_ref), (log_in, log_ref),
        (lat_in, lat_ref), (w_in, w_ref), (rot_in, rot_ref),
    )
    fetch = [pltpu.make_async_copy(u, v, loads.at[i]) for i, (u, v) in enumerate(pairs)]
    for f in fetch:
        f.start()
    for d in far:
        greet(at_z(partner(H, a, d, 1)))
    repeat(1, GY, lambda e: greet(at_y(e)))
    repeat(1, GX, lambda e: greet(at_x(e)))
    repeat(1, TP, greet_tp)

    def copy(src, dst, ssem, rsem, sp):
        return pltpu.make_async_remote_copy(
            src_ref=src, dst_ref=dst, send_sem=ssem, recv_sem=rsem,
            device_id={"sp": sp}, device_id_type=MESH,
        )

    def copy_tp(src, dst, ssem, rsem, i):
        return pltpu.make_async_remote_copy(
            src_ref=src, dst_ref=dst, send_sem=ssem, recv_sem=rsem,
            device_id={"tp": lax.rem(tpi + i, TP)}, device_id_type=MESH,
        )

    for f in fetch[:4]:
        f.wait()
    prod = out_ref[...].astype(F32) * go_ref[...].astype(F32)
    high = prod.astype(BF16)
    rest = (prod - high.astype(F32)).astype(BF16)
    head_of = lax.broadcasted_iota(jnp.int32, (8 * -(-H // 8), H * VDIM), 1) // VDIM
    picks = (head_of == lax.broadcasted_iota(jnp.int32, head_of.shape, 0)).astype(F32).astype(BF16)
    deltas = dot(picks, high, ((1,), (1,))) + dot(picks, rest, ((1,), (1,)))
    logs = log_ref[...] * log2e
    for j in range(H):
        start = HEAD * j
        qs[j, :T, :] = jnp.concatenate(
            [q_ref[:, start : start + NOPE], go_ref[:, VDIM * j : VDIM * (j + 1)]], axis=1)
        turned = q_ref[:, start + NOPE : start + HEAD]
        qs[j, T : T + quarter, :] = jnp.concatenate(
            [turned[quarter * i : quarter * (i + 1)] for i in range(LANES // ROPE)], axis=1)
        terms = three_terms(logs[j : j + 1]) + three_terms(deltas[j : j + 1])
        qs[j, T + quarter :, :] = jnp.concatenate(
            [t.astype(F32) for t in terms] + [jnp.zeros((STATS - 6, T), F32)], axis=0).astype(BF16)
    wq[y, a] = qs[a]
    pl.semaphore_wait(barrier, H - 1 + GY - 1 + GX - 1 + TP - 1)

    def first_q(d):
        to = partner(H, a, d, 1)
        return copy(qs.at[to], wq.at[y, a], s1q.at[d - 1], r1q.at[d - 1], at_z(to))

    def first_k(d):
        to = partner(H, a, d, 1)
        return copy(pk.at[to], kb.at[x, a], s1k.at[d - 1], r1k.at[d - 1], at_z(to))

    def relay_q(d, e):
        src = wq.at[y, partner(H, a, d, -1)]
        return copy(src, src, s2q.at[e - 1, d], r2q.at[e - 1, d], at_y(e))

    def relay_k(d, e):
        src = kb.at[x, partner(H, a, d, -1)]
        return copy(src, src, s2k.at[e - 1, d], r2k.at[e - 1, d], at_x(e))

    for d in far:
        first_q(d).start()
    repeat(1, GY, lambda e: relay_q(0, e).start())
    for f in fetch[4:]:
        f.wait()
    joined = dot(lat_ref[...], w_ref[...], ((1,), (0,))).astype(BF16)
    for j in range(H):
        pk[j, :T, :] = joined[:, LANES * j : LANES * (j + 1)]
        pk[j, T:, :] = rot_ref[...]
    kb[x, a] = pk[a]
    for d in far:
        first_k(d).start()
    repeat(1, GX, lambda e: relay_k(0, e).start())
    lb[a] = lat_ref[...].reshape(lb.shape[1:])
    for d in far:
        first_q(d).wait_recv()
        repeat(1, GY, lambda e: relay_q(d, e).start())
    for d in far:
        first_k(d).wait_recv()
        repeat(1, GX, lambda e: relay_k(d, e).start())

    slab = T // TP
    mine = lat_ref.at[pl.ds(pl.multiple_of(tpi * slab, slab), slab)]

    def first_l(d):
        return copy(mine, lb.at[a, tpi], s1l.at[d - 1], r1l.at[d - 1], at_z(partner(H, a, d, 1)))

    def hand_on(d, i):
        piece = lb.at[partner(H, a, d, -1), tpi]
        return copy_tp(piece, piece, s8.at[d - 1, i - 1], r8.at[d - 1, i - 1], i)

    for d in far:
        first_l(d).start()

    many = GY * H * T

    def keys_of(where, units):
        tall, wide, turned = [], [], []
        for u in units:
            kv = kb[where, u, :T, :]
            rot = kb[where, u, T:, :]
            lane = lax.broadcasted_iota(jnp.int32, (T, LANES), 1)
            part = jnp.where(lane < NOPE, kv, jnp.zeros_like(kv))
            column = rot.astype(F32).T.astype(BF16)
            tall.append(jnp.concatenate([part, column, jnp.zeros((T, LANES - ROPE), BF16)], axis=1))
            wide.append(kv - part)
            turned.append(jnp.concatenate([kv.astype(F32).T.astype(BF16)[:NOPE], rot], axis=0))
        return jnp.concatenate(tall, axis=0), jnp.concatenate(wide, axis=0), jnp.concatenate(turned, axis=1)

    def attend(where, units):
        key, value, turned = keys_of(where, units)
        row = wq[:, :, :T, :].reshape(many, LANES)
        both = jnp.concatenate([row, rp[...]], axis=1)
        stats = [wq[i, j, T + quarter :, :].astype(F32) for i in range(GY) for j in range(H)]
        log = jnp.concatenate([t[0:1] + t[1:2] + t[2:3] for t in stats], axis=1)
        delta = jnp.concatenate([t[3:4] + t[4:5] + t[5:6] for t in stats], axis=1)
        s = dot(key, both, ((1,), (1,)))
        dp = dot(value, row, ((1,), (1,)))
        p = jnp.exp2(s * (scale * log2e) - log)
        ds = (p * (dp - delta)).astype(BF16)
        dq = dot(turned, ds, ((1,), (0,)))
        dk = dot(ds, both, ((1,), (0,))) * scale
        dv = dot(p.astype(BF16), row, ((1,), (0,)))
        lane = lax.broadcasted_iota(jnp.int32, dv.shape, 1)
        return dq, jnp.where(lane < NOPE, dk[:, :LANES], dv), dk[:, LANES:].T[:ROPE]

    for e in range(1, GY):
        for d in [0] + far:
            relay_q(d, e).wait_recv()
    for i in range(GY):
        for j in range(H):
            packed = wq[i, j, T : T + quarter, :]
            base = (i * H + j) * T
            for k in range(LANES // ROPE):
                part = packed if k == 0 else jnp.concatenate(
                    [packed[:, ROPE * k :], packed[:, : ROPE * k]], axis=1)
                rp[base + quarter * k : base + quarter * (k + 1), :] = part

    every = range(H)
    dq, kv, rot = attend(x, every)
    wide = H * T
    for i in range(GY):
        dqa[i] = dq[:, wide * i : wide * (i + 1)]
    own_kv[...] = kv
    own_rot[...] = rot

    order = [0] + far
    chunk = 2 if H % 2 == 0 else 1

    def back_k(e, n):
        piece = pl.ds(n * chunk, chunk)
        return copy(kvs.at[e - 1, piece], kvr.at[e - 1, piece], s3k.at[e - 1, n], r3k.at[e - 1, n], at_x(e))

    def unit_of(n, c, sign):
        return partner(H, a, order[n * chunk + c], sign)

    for e in range(1, GX):
        where = lax.rem(x + e, GX)
        for n in range(H // chunk):
            units = [unit_of(n, c, -1) for c in range(chunk)]
            for c in range(chunk):
                relay_k(order[n * chunk + c], GX - e).wait_recv()
            dq, kv, rot = attend(where, units)
            for c in range(chunk):
                kvs[e - 1, n * chunk + c, :T, :] = kv[T * c : T * (c + 1)].astype(KV_PART)
                kvs[e - 1, n * chunk + c, T:, :] = rot[:, T * c : T * (c + 1)].astype(KV_PART)
            back_k(e, n).start()
            for i in range(GY):
                dqa[i] += dq[:, wide * i : wide * (i + 1)]

    def back_q(e):
        return copy(dqs.at[e - 1], dqr.at[e - 1], s3q.at[e - 1], r3q.at[e - 1], at_y(e))

    for e in range(1, GY):
        dqs[e - 1] = dqa[lax.rem(y + e, GY)].astype(DQ_PART)
        back_q(e).start()

    for d in far:
        first_l(d).wait_recv()
        repeat(1, TP, lambda i: hand_on(d, i).start())

    def home_k(d):
        to = partner(H, a, d, 1)
        return copy(kvo.at[to], kvh.at[a], s4k.at[d - 1], r4k.at[d - 1], at_z(to))

    def home_r(d):
        to = partner(H, a, d, 1)
        return copy(ro.at[to], rr.at[a], s4r.at[d - 1], r4r.at[d - 1], at_z(to))

    for n in range(H // chunk):
        for e in range(1, GX):
            back_k(e, n).wait_recv()
        for c in range(chunk):
            slot = n * chunk + c
            u = unit_of(n, c, -1)
            place = pl.ds(pl.multiple_of(u * T, T), T)
            kvo[u] = (own_kv[place, :] + add_all([kvr[e - 1, slot, :T, :].astype(F32) for e in range(1, GX)])
                      if GX > 1 else own_kv[place, :]).astype(BF16)
            turn = own_rot[:, place]
            ro[u] = turn + add_all([kvr[e - 1, slot, T:, :].astype(F32) for e in range(1, GX)]) if GX > 1 else turn

    for d in far:
        home_k(d).start()
    kvh[a] = kvo[a]
    rr[a] = ro[a]

    for d in far:
        repeat(1, TP, lambda i: hand_on(d, i).wait_recv())
    lat = lb[...].reshape(wide, lb.shape[3])
    total = dot(lat, kvo[...].reshape(wide, LANES), ((0,), (0,)))
    rows = wgs.shape[1]
    wgs[...] = total.reshape(S, rows, LANES).astype(WG_PART)
    wgr[me] = wgs[me]

    def share(i):
        to = lax.rem(me + i, S)
        return copy(wgs.at[to], wgr.at[me], s5.at[i - 1], r5.at[i - 1], to)

    def spread(i, carry):
        share(i).start()
        return carry

    lax.fori_loop(1, S, spread, 0)
    for d in far:
        home_r(d).start()

    mine_q = dqa[y]
    for e in range(1, GY):
        back_q(e).wait_recv()
        mine_q = mine_q + dqr[e - 1].astype(F32)
    mine_q = (mine_q * scale).astype(BF16)
    for j in range(H):
        dqo[j] = mine_q[:, T * j : T * (j + 1)]

    def home_q(d):
        to = partner(H, a, d, 1)
        return copy(dqo.at[to], dqh.at[a], s4q.at[d - 1], r4q.at[d - 1], at_z(to))

    for d in far:
        home_q(d).start()
    dqh[a] = dqo[a]

    for d in far:
        home_k(d).wait_recv()
    for j in range(H):
        kg_ref[:, NOPE * j : NOPE * (j + 1)] = kvh[j, :, :NOPE]
        vg_ref[:, VDIM * j : VDIM * (j + 1)] = kvh[j, :, NOPE:]
    for d in far:
        home_r(d).wait_recv()
    rt[tpi] = add_all([rr[j] for j in range(H)])

    def swap(i):
        return copy_tp(rt.at[tpi], rt.at[tpi], s6.at[i - 1], r6.at[i - 1], i)

    repeat(1, TP, lambda i: swap(i).start())
    for d in far:
        home_q(d).wait_recv()
    qg_ref[...] = dqh[...].reshape(H * HEAD, T).astype(F32).T.astype(BF16)
    repeat(1, TP, lambda i: swap(i).wait_recv())
    rg_ref[...] = add_all([rt[i] for i in range(TP)])

    def arrive(i, carry):
        share(i).wait_recv()
        return carry

    lax.fori_loop(1, S, arrive, 0)
    for j in range(H):
        wg_ref[:, LANES * j : LANES * (j + 1)] = add_all([wgr[j * G + i].astype(F32) for i in range(G)])

    for d in far:
        for c in (first_q(d), first_k(d), first_l(d), home_k(d), home_r(d), home_q(d)):
            c.wait_send()
        repeat(1, TP, lambda i: hand_on(d, i).wait_send())
    for d in order:
        repeat(1, GY, lambda e: relay_q(d, e).wait_send())
        repeat(1, GX, lambda e: relay_k(d, e).wait_send())
    for n in range(H // chunk):
        repeat(1, GX, lambda e: back_k(e, n).wait_send())
    repeat(1, GY, lambda e: back_q(e).wait_send())
    repeat(1, TP, lambda i: swap(i).wait_send())

    def left(i, carry):
        share(i).wait_send()
        return carry

    lax.fori_loop(1, S, left, 0)


def put_out(*refs):
    copies = [pltpu.make_async_copy(refs[i], refs[5 + i], refs[10].at[i]) for i in range(5)]
    for c in copies:
        c.start()
    for c in copies:
        c.wait()


def per_device(S, TP, queries, latents, rot_key, kv_weight, log_sums, outputs, out_grad):
    T, rank = latents.shape
    H = log_sums.shape[1]
    G = S // H
    GX = max(d for d in range(1, math.isqrt(G) + 1) if G % d == 0)
    GY = G // GX
    rows = rank // S
    wide = H * T
    dma = lambda *n: pltpu.SemaphoreType.DMA(tuple(max(k, 1) for k in n))
    pairs = lambda *n: [dma(*n), dma(*n)]
    vm = lambda shape, kind: pltpu.VMEM(tuple(max(k, 1) for k in shape), kind)
    unit = T + T * ROPE // LANES + STATS
    arrays = (queries, latents, rot_key.T, kv_weight, log_sums.T, outputs, out_grad)
    scratch = [
        *[vm(u.shape, u.dtype) for u in arrays], dma(len(arrays)),
        vm((H, unit, LANES), BF16), vm((H, T + ROPE, LANES), BF16),
        vm((GY, H, unit, LANES), BF16), vm((GX, H, T + ROPE, LANES), BF16), vm((H, TP, T // TP, rank), BF16),
        vm((GY * wide, LANES), BF16), vm((GY, HEAD, wide), F32),
        *[vm((GY - 1, HEAD, wide), DQ_PART)] * 2, *[vm((GX - 1, H, T + ROPE, LANES), KV_PART)] * 2,
        vm((wide, LANES), F32), vm((ROPE, wide), F32),
        *[vm((H, T, LANES), BF16)] * 2, *[vm((H, ROPE, T), F32)] * 2, vm((TP, ROPE, T), F32),
        *[vm((S, rows, LANES), WG_PART)] * 2, *[vm((H, HEAD, T), BF16)] * 2,
        *pairs(H - 1), *pairs(H - 1), *pairs(H - 1), *pairs(GY - 1, H), *pairs(GX - 1, H),
        *pairs(GY - 1), *pairs(GX - 1, H),
        *pairs(H - 1), *pairs(H - 1), *pairs(H - 1), *pairs(S - 1), *pairs(TP - 1), *pairs(H - 1, TP - 1),
    ]
    shapes = [
        ((T, H * HEAD), BF16), ((T, H * NOPE), BF16), ((T, H * VDIM), BF16),
        ((ROPE, T), F32), ((rows, H * LANES), F32),
    ]
    held = sum(u[0] * -(-u[1] // LANES) * LANES * jnp.dtype(t).itemsize for u, t in shapes)
    results = pl.pallas_call(
        functools.partial(kernel, S, TP, H, GY, GX),
        out_shape=[pltpu.VMEM(*u) for u in shapes],
        in_specs=[pl.BlockSpec(memory_space=pltpu.HBM)] * 7,
        out_specs=[pl.BlockSpec(memory_space=pltpu.VMEM)] * 5,
        scratch_shapes=scratch,
        compiler_params=pltpu.CompilerParams(
            collective_id=0, has_side_effects=True, vmem_limit_bytes=VMEM_BYTES - held - SPARE
        ),
    )(*arrays)
    query_grad, key_grad, value_grad, rot_grad, weight_grad = pl.pallas_call(
        put_out,
        out_shape=[jax.ShapeDtypeStruct(*u) for u in shapes],
        in_specs=[pl.BlockSpec(memory_space=pltpu.VMEM)] * 5,
        out_specs=[pl.BlockSpec(memory_space=pltpu.HBM)] * 5,
        scratch_shapes=[dma(5)],
        compiler_params=pltpu.CompilerParams(vmem_limit_bytes=1 << 20),
    )(*results)
    return query_grad, key_grad, value_grad, rot_grad.T, weight_grad


def solution(mesh):
    placed = (
        P("sp", "tp"), P("sp", None), P("sp", None), P(None, "tp"),
        P("sp", "tp"), P("sp", "tp"), P("sp", "tp"),
    )
    return jax.shard_map(
        functools.partial(per_device, mesh.shape["sp"], mesh.shape["tp"]),
        mesh=mesh,
        in_specs=placed,
        out_specs=(P("sp", "tp"), P("sp", "tp"), P("sp", "tp"), P("sp", None), P("sp", "tp")),
        check_vma=False,
    )
```

time: 38.8 us -> 34.7 us (0.89)
  Pallas kernels: 38 us -> 33.9 us
    pallas_call x2, Pallas kernels: 38 us -> 33.9 us  [the longest x1 33.2 us: per_device(): pl.pallas_call(functools.partial(kernel, S, TP, H, GY, GX), out_shape=[pl...]
where the time goes in v1:
time: 34.7 us; the launch traced here: 34.6 us
  Pallas kernels  33.9 us (98%)
  between operations  0.64 us (2%)
    pallas_call x1, Pallas kernels, per_device(): pl.pallas_call(functools.partial(kernel, S, TP, H, GY, GX), out_shape=[pl...  33.2 us
    pallas_call x1, Pallas kernels, per_device(): pl.pallas_call(put_out, out_shape=[jax.ShapeDtypeStruct(*u) for u in shap...  0.76 us

profile of v1, /device:TPU:0, one launch (start us, length us, event | category | flops | bytes accessed | tf_op | source)
XLA Modules:
  0.0 34.6 jit_solution(1176421047929325875)
XLA Ops:
  0.6 33.2 %shard_map.110 = (bf16[128,384]{1,0:T(8,128)(2,1)S(1)}, bf16[128,256]{1,0:T(8,128)(2,1)S(1)}, bf16[128,256]{1,0:T(8,128)(2,1)S(1)}, f32[32,128]{1,0:T(8,128)S(1)}, f32[32,512]{1,0:T(8,128)S(1)}) custom-call(bf16[128,384]{1,0:T(8,128)(2,1)} %q_in.1, bf16[128,512]{1,0:T(8,128)(2,1)} %lat_in.1, bf16[32,128]{1,0:T(8,128)(2,1)} %bitcast.3, ...), custom_call_target="tpu_custom_call" | custom-call | tf_op jit(solution)/shard_map/pallas_call | solution.py:445
  33.8 0.8 %shard_map.111 = (bf16[128,384]{1,0:T(8,128)(2,1)}, bf16[128,256]{1,0:T(8,128)(2,1)}, bf16[128,256]{1,0:T(8,128)(2,1)}, f32[32,128]{1,0:T(8,128)}, f32[32,512]{1,0:T(8,128)}) custom-call(bf16[128,384]{1,0:T(8,128)(2,1)S(1)} %get-tuple-element.15.refs_0_, bf16[128,256]{1,0:T(8,128)(2,1)S(1)} %get-tuple-element.16.refs_1_, ...), custom_call_target="tpu_custom_call" | custom-call | tf_op jit(solution)/shard_map/pallas_call | solution.py:455

commit v2 on v1

--- a/solution.py
+++ b/solution.py
@@ -20,7 +20,7 @@
 F32 = jnp.float32
 BF16 = jnp.bfloat16
 KV_PART = BF16
-DQ_PART = F32
+DQ_PART = BF16
 WG_PART = BF16
 
 
@@ -71,7 +71,7 @@
 def distances(n):
     if not power_of_two(n):
         return list(range(1, n))
-    return list(range(n // 2, n)) + list(range(1, n // 2))
+    return sorted(range(1, n), key=lambda d: -bin(d).count("1"))
 
 
 def kernel(
@@ -79,7 +79,7 @@
     q_in, lat_in, rot_in, w_in, log_in, out_in, go_in,
     qg_ref, kg_ref, vg_ref, rg_ref, wg_ref,
     q_ref, lat_ref, rot_ref, w_ref, log_ref, out_ref, go_ref, loads,
-    qs, pk, wq, kb, lb, rp, dqa, dqs, dqr, kvs, kvr, own_kv, own_rot,
+    qs, pk, wq, kb, lb, rp, dqa, dqs, dqr, kvs, kvr, dka, dva,
     kvo, kvh, ro, rr, rt, wgs, wgr, dqo, dqh,
     s1q, r1q, s1k, r1k, s1l, r1l, s2q, r2q, s2k, r2k, s3q, r3q, s3k, r3k,
     s4q, r4q, s4k, r4k, s4r, r4r, s5, r5, s6, r6, s8, r8,
@@ -88,7 +88,7 @@
     T = q_ref.shape[0]
     me = lax.axis_index("sp")
     tpi = lax.axis_index("tp")
-    a, b = me // G, lax.rem(me, G)
+    a, b = lax.rem(me, H), me // H
     y, x = b // GX, lax.rem(b, GX)
     scale = HEAD ** (-0.5)
     log2e = math.log2(math.e)
@@ -103,14 +103,14 @@
     def greet_tp(i):
         pl.semaphore_signal(barrier, inc=1, device_id={"tp": lax.rem(tpi + i, TP)}, device_id_type=MESH)
 
-    def at_z(z):
-        return z * G + b
+    def at_a(z):
+        return b * H + z
 
     def at_y(e):
-        return a * G + lax.rem(y + e, GY) * GX + x
+        return (lax.rem(y + e, GY) * GX + x) * H + a
 
     def at_x(e):
-        return a * G + y * GX + lax.rem(x + e, GX)
+        return (y * GX + lax.rem(x + e, GX)) * H + a
 
     pairs = (
         (q_in, q_ref), (go_in, go_ref), (out_in, out_ref), (log_in, log_ref),
@@ -120,7 +120,7 @@
     for f in fetch:
         f.start()
     for d in far:
-        greet(at_z(partner(H, a, d, 1)))
+        greet(at_a(partner(H, a, d, 1)))
     repeat(1, GY, lambda e: greet(at_y(e)))
     repeat(1, GX, lambda e: greet(at_x(e)))
     repeat(1, TP, greet_tp)
@@ -161,11 +161,11 @@
 
     def first_q(d):
         to = partner(H, a, d, 1)
-        return copy(qs.at[to], wq.at[y, a], s1q.at[d - 1], r1q.at[d - 1], at_z(to))
+        return copy(qs.at[to], wq.at[y, a], s1q.at[d - 1], r1q.at[d - 1], at_a(to))
 
     def first_k(d):
         to = partner(H, a, d, 1)
-        return copy(pk.at[to], kb.at[x, a], s1k.at[d - 1], r1k.at[d - 1], at_z(to))
+        return copy(pk.at[to], kb.at[x, a], s1k.at[d - 1], r1k.at[d - 1], at_a(to))
 
     def relay_q(d, e):
         src = wq.at[y, partner(H, a, d, -1)]
@@ -200,7 +200,7 @@
     mine = lat_ref.at[pl.ds(pl.multiple_of(tpi * slab, slab), slab)]
 
     def first_l(d):
-        return copy(mine, lb.at[a, tpi], s1l.at[d - 1], r1l.at[d - 1], at_z(partner(H, a, d, 1)))
+        return copy(mine, lb.at[a, tpi], s1l.at[d - 1], r1l.at[d - 1], at_a(partner(H, a, d, 1)))
 
     def hand_on(d, i):
         piece = lb.at[partner(H, a, d, -1), tpi]
@@ -209,9 +209,8 @@
     for d in far:
         first_l(d).start()
 
-    many = GY * H * T
-
-    def keys_of(where, units):
+    def keys_of(e, units):
+        where = lax.rem(x + e, GX)
         tall, wide, turned = [], [], []
         for u in units:
             kv = kb[where, u, :T, :]
@@ -224,11 +223,26 @@
             turned.append(jnp.concatenate([kv.astype(F32).T.astype(BF16)[:NOPE], rot], axis=0))
         return jnp.concatenate(tall, axis=0), jnp.concatenate(wide, axis=0), jnp.concatenate(turned, axis=1)
 
-    def attend(where, units):
-        key, value, turned = keys_of(where, units)
-        row = wq[:, :, :T, :].reshape(many, LANES)
-        both = jnp.concatenate([row, rp[...]], axis=1)
-        stats = [wq[i, j, T + quarter :, :].astype(F32) for i in range(GY) for j in range(H)]
+    wide = H * T
+    order = [0] + far
+    chunk = 2 if H % 2 == 0 else 1
+    chunks = H // chunk
+
+    def prepare(f):
+        col = lax.rem(y + f, GY)
+        for j in range(H):
+            packed = wq[col, j, T : T + quarter, :]
+            for k in range(LANES // ROPE):
+                part = packed if k == 0 else jnp.concatenate(
+                    [packed[:, ROPE * k :], packed[:, : ROPE * k]], axis=1)
+                rp[f, T * j + quarter * k : T * j + quarter * (k + 1), :] = part
+
+    def attend(keys, f):
+        key, value, turned = keys
+        col = lax.rem(y + f, GY)
+        row = wq[col, :, :T, :].reshape(wide, LANES)
+        both = jnp.concatenate([row, rp[f]], axis=1)
+        stats = [wq[col, j, T + quarter :, :].astype(F32) for j in range(H)]
         log = jnp.concatenate([t[0:1] + t[1:2] + t[2:3] for t in stats], axis=1)
         delta = jnp.concatenate([t[3:4] + t[4:5] + t[5:6] for t in stats], axis=1)
         s = dot(key, both, ((1,), (1,)))
@@ -236,95 +250,123 @@
         p = jnp.exp2(s * (scale * log2e) - log)
         ds = (p * (dp - delta)).astype(BF16)
         dq = dot(turned, ds, ((1,), (0,)))
-        dk = dot(ds, both, ((1,), (0,))) * scale
+        dk = dot(ds, both, ((1,), (0,)))
         dv = dot(p.astype(BF16), row, ((1,), (0,)))
+        return dq, dk, dv
+
+    def unit_of(k, sign):
+        return partner(H, a, order[k], sign)
+
+    def span(n):
+        return pl.ds(wide // chunks * n, wide // chunks)
+
+    def keys_at(e, n):
+        return keys_of(e, [unit_of(n * chunk + c, -1) for c in range(chunk)])
+
+    def whole_keys(e):
+        return keys_of(e, [unit_of(k, -1) for k in range(H)])
+
+    def gather(e, n, dk, dv, first):
+        if first:
+            dka[e, span(n), :] = dk
+            dva[e, span(n), :] = dv
+        else:
+            dka[e, span(n), :] += dk
+            dva[e, span(n), :] += dv
+
+    def gather_all(e, dk, dv, first):
+        for n in range(chunks):
+            part = slice(wide // chunks * n, wide // chunks * (n + 1))
+            gather(e, n, dk[part], dv[part], first)
+
+    def totals(e, n):
+        dk, dv = dka[e, span(n), :], dva[e, span(n), :]
         lane = lax.broadcasted_iota(jnp.int32, dv.shape, 1)
-        return dq, jnp.where(lane < NOPE, dk[:, :LANES], dv), dk[:, LANES:].T[:ROPE]
-
-    for e in range(1, GY):
-        for d in [0] + far:
-            relay_q(d, e).wait_recv()
-    for i in range(GY):
-        for j in range(H):
-            packed = wq[i, j, T : T + quarter, :]
-            base = (i * H + j) * T
-            for k in range(LANES // ROPE):
-                part = packed if k == 0 else jnp.concatenate(
-                    [packed[:, ROPE * k :], packed[:, : ROPE * k]], axis=1)
-                rp[base + quarter * k : base + quarter * (k + 1), :] = part
-
-    every = range(H)
-    dq, kv, rot = attend(x, every)
-    wide = H * T
-    for i in range(GY):
-        dqa[i] = dq[:, wide * i : wide * (i + 1)]
-    own_kv[...] = kv
-    own_rot[...] = rot
-
-    order = [0] + far
-    chunk = 2 if H % 2 == 0 else 1
+        dk = dk * scale
+        return jnp.where(lane < NOPE, dk[:, :LANES], dv), dk[:, LANES:].T[:ROPE]
 
     def back_k(e, n):
         piece = pl.ds(n * chunk, chunk)
         return copy(kvs.at[e - 1, piece], kvr.at[e - 1, piece], s3k.at[e - 1, n], r3k.at[e - 1, n], at_x(e))
 
-    def unit_of(n, c, sign):
-        return partner(H, a, order[n * chunk + c], sign)
-
+    def back_q(f):
+        return copy(dqs.at[f - 1], dqr.at[f - 1], s3q.at[f - 1], r3q.at[f - 1], at_y(f))
+
+    def send_k(e, n):
+        kv, rot = totals(e, n)
+        for c in range(chunk):
+            kvs[e - 1, n * chunk + c, :T, :] = kv[T * c : T * (c + 1)].astype(KV_PART)
+            kvs[e - 1, n * chunk + c, T:, :] = rot[:, T * c : T * (c + 1)].astype(KV_PART)
+        back_k(e, n).start()
+
+    prepare(0)
+    dq, dk, dv = attend(whole_keys(0), 0)
+    dqa[0] = dq
+    gather_all(0, dk, dv, True)
     for e in range(1, GX):
-        where = lax.rem(x + e, GX)
-        for n in range(H // chunk):
-            units = [unit_of(n, c, -1) for c in range(chunk)]
-            for c in range(chunk):
-                relay_k(order[n * chunk + c], GX - e).wait_recv()
-            dq, kv, rot = attend(where, units)
-            for c in range(chunk):
-                kvs[e - 1, n * chunk + c, :T, :] = kv[T * c : T * (c + 1)].astype(KV_PART)
-                kvs[e - 1, n * chunk + c, T:, :] = rot[:, T * c : T * (c + 1)].astype(KV_PART)
-            back_k(e, n).start()
-            for i in range(GY):
-                dqa[i] += dq[:, wide * i : wide * (i + 1)]
-
-    def back_q(e):
-        return copy(dqs.at[e - 1], dqr.at[e - 1], s3q.at[e - 1], r3q.at[e - 1], at_y(e))
-
-    for e in range(1, GY):
-        dqs[e - 1] = dqa[lax.rem(y + e, GY)].astype(DQ_PART)
-        back_q(e).start()
+        for d in order:
+            relay_k(d, GX - e).wait_recv()
+        dq, dk, dv = attend(whole_keys(e), 0)
+        dqa[0] += dq
+        gather_all(e, dk, dv, True)
+    for f in range(1, GY):
+        for d in order:
+            relay_q(d, GY - f).wait_recv()
+        prepare(f)
+        for e in range(1, GX):
+            for n in range(chunks):
+                dq, dk, dv = attend(keys_at(e, n), f)
+                if e == 1 and n == 0:
+                    dqa[f] = dq
+                else:
+                    dqa[f] += dq
+                gather(e, n, dk, dv, False)
+                if f == GY - 1:
+                    send_k(e, n)
+        dq, dk, dv = attend(whole_keys(0), f)
+        dqs[f - 1] = (dqa[f] + dq if GX > 1 else dq).astype(DQ_PART)
+        back_q(f).start()
+        gather_all(0, dk, dv, False)
 
     for d in far:
         first_l(d).wait_recv()
         repeat(1, TP, lambda i: hand_on(d, i).start())
 
     def home_k(d):
-        to = partner(H, a, d, 1)
-        return copy(kvo.at[to], kvh.at[a], s4k.at[d - 1], r4k.at[d - 1], at_z(to))
+        to = partner(H, a, d, -1)
+        return copy(kvo.at[order.index(d)], kvh.at[a], s4k.at[d - 1], r4k.at[d - 1], at_a(to))
 
     def home_r(d):
-        to = partner(H, a, d, 1)
-        return copy(ro.at[to], rr.at[a], s4r.at[d - 1], r4r.at[d - 1], at_z(to))
-
-    for n in range(H // chunk):
+        to = partner(H, a, d, -1)
+        return copy(ro.at[order.index(d)], rr.at[a], s4r.at[d - 1], r4r.at[d - 1], at_a(to))
+
+    for d in far:
+        repeat(1, TP, lambda i: hand_on(d, i).wait_recv())
+    grads = []
+    for n in range(chunks):
         for e in range(1, GX):
             back_k(e, n).wait_recv()
+        kv, rot = totals(0, n)
+        lats, finals = [], []
         for c in range(chunk):
             slot = n * chunk + c
-            u = unit_of(n, c, -1)
-            place = pl.ds(pl.multiple_of(u * T, T), T)
-            kvo[u] = (own_kv[place, :] + add_all([kvr[e - 1, slot, :T, :].astype(F32) for e in range(1, GX)])
-                      if GX > 1 else own_kv[place, :]).astype(BF16)
-            turn = own_rot[:, place]
-            ro[u] = turn + add_all([kvr[e - 1, slot, T:, :].astype(F32) for e in range(1, GX)]) if GX > 1 else turn
-
-    for d in far:
-        home_k(d).start()
-    kvh[a] = kvo[a]
-    rr[a] = ro[a]
-
-    for d in far:
-        repeat(1, TP, lambda i: hand_on(d, i).wait_recv())
-    lat = lb[...].reshape(wide, lb.shape[3])
-    total = dot(lat, kvo[...].reshape(wide, LANES), ((0,), (0,)))
+            u = unit_of(slot, -1)
+            part, turn = kv[T * c : T * (c + 1)], rot[:, T * c : T * (c + 1)]
+            for e in range(1, GX):
+                part = part + kvr[e - 1, slot, :T, :].astype(F32)
+                turn = turn + kvr[e - 1, slot, T:, :].astype(F32)
+            part = part.astype(BF16)
+            kvo[slot] = part
+            ro[slot] = turn
+            lats.append(lb[u].reshape(T, lb.shape[3]))
+            finals.append(part)
+            if slot == 0:
+                kvh[a] = part
+                rr[a] = turn
+            else:
+                home_k(order[slot]).start()
+        grads.append(dot(jnp.concatenate(lats, axis=0), jnp.concatenate(finals, axis=0), ((0,), (0,))))
+    total = add_all(grads)
     rows = wgs.shape[1]
     wgs[...] = total.reshape(S, rows, LANES).astype(WG_PART)
     wgr[me] = wgs[me]
@@ -341,7 +383,7 @@
     for d in far:
         home_r(d).start()
 
-    mine_q = dqa[y]
+    mine_q = dqa[0]
     for e in range(1, GY):
         back_q(e).wait_recv()
         mine_q = mine_q + dqr[e - 1].astype(F32)
@@ -351,7 +393,7 @@
 
     def home_q(d):
         to = partner(H, a, d, 1)
-        return copy(dqo.at[to], dqh.at[a], s4q.at[d - 1], r4q.at[d - 1], at_z(to))
+        return copy(dqo.at[to], dqh.at[a], s4q.at[d - 1], r4q.at[d - 1], at_a(to))
 
     for d in far:
         home_q(d).start()
@@ -382,7 +424,7 @@
 
     lax.fori_loop(1, S, arrive, 0)
     for j in range(H):
-        wg_ref[:, LANES * j : LANES * (j + 1)] = add_all([wgr[j * G + i].astype(F32) for i in range(G)])
+        wg_ref[:, LANES * j : LANES * (j + 1)] = add_all([wgr[i * H + j].astype(F32) for i in range(G)])
 
     for d in far:
         for c in (first_q(d), first_k(d), first_l(d), home_k(d), home_r(d), home_q(d)):
@@ -391,7 +433,7 @@
     for d in order:
         repeat(1, GY, lambda e: relay_q(d, e).wait_send())
         repeat(1, GX, lambda e: relay_k(d, e).wait_send())
-    for n in range(H // chunk):
+    for n in range(chunks):
         repeat(1, GX, lambda e: back_k(e, n).wait_send())
     repeat(1, GY, lambda e: back_q(e).wait_send())
     repeat(1, TP, lambda i: swap(i).wait_send())
@@ -428,9 +470,9 @@
         *[vm(u.shape, u.dtype) for u in arrays], dma(len(arrays)),
         vm((H, unit, LANES), BF16), vm((H, T + ROPE, LANES), BF16),
         vm((GY, H, unit, LANES), BF16), vm((GX, H, T + ROPE, LANES), BF16), vm((H, TP, T // TP, rank), BF16),
-        vm((GY * wide, LANES), BF16), vm((GY, HEAD, wide), F32),
+        vm((GY, wide, LANES), BF16), vm((GY, HEAD, wide), F32),
         *[vm((GY - 1, HEAD, wide), DQ_PART)] * 2, *[vm((GX - 1, H, T + ROPE, LANES), KV_PART)] * 2,
-        vm((wide, LANES), F32), vm((ROPE, wide), F32),
+        vm((GX, wide, 2 * LANES), F32), vm((GX, wide, LANES), F32),
         *[vm((H, T, LANES), BF16)] * 2, *[vm((H, ROPE, T), F32)] * 2, vm((TP, ROPE, T), F32),
         *[vm((S, rows, LANES), WG_PART)] * 2, *[vm((H, HEAD, T), BF16)] * 2,
         *pairs(H - 1), *pairs(H - 1), *pairs(H - 1), *pairs(GY - 1, H), *pairs(GX - 1, H),

time: 34.7 us -> 30.3 us (0.87)
  Pallas kernels: 33.9 us -> 29.5 us
    pallas_call x1, Pallas kernels: 33.2 us -> 28.7 us  [per_device(): pl.pallas_call(functools.partial(kernel, S, TP, H, GY, GX), out_shape=[pl...]
where the time goes in v2:
time: 30.3 us; the launch traced here: 30.1 us
  Pallas kernels  29.5 us (97%)
  between operations  0.64 us (2%)
    pallas_call x1, Pallas kernels, per_device(): pl.pallas_call(functools.partial(kernel, S, TP, H, GY, GX), out_shape=[pl...  28.7 us
    pallas_call x1, Pallas kernels, per_device(): pl.pallas_call(put_out, out_shape=[jax.ShapeDtypeStruct(*u) for u in shap...  0.76 us

profile of v2, /device:TPU:0, one launch (start us, length us, event | category | flops | bytes accessed | tf_op | source)
XLA Modules:
  0.0 30.1 jit_solution(13371686154094902279)
XLA Ops:
  0.6 28.7 %shard_map.110 = (bf16[128,384]{1,0:T(8,128)(2,1)S(1)}, bf16[128,256]{1,0:T(8,128)(2,1)S(1)}, bf16[128,256]{1,0:T(8,128)(2,1)S(1)}, f32[32,128]{1,0:T(8,128)S(1)}, f32[32,512]{1,0:T(8,128)S(1)}) custom-call(bf16[128,384]{1,0:T(8,128)(2,1)} %q_in.1, bf16[128,512]{1,0:T(8,128)(2,1)} %lat_in.1, bf16[32,128]{1,0:T(8,128)(2,1)} %bitcast.3, ...), custom_call_target="tpu_custom_call" | custom-call | tf_op jit(solution)/shard_map/pallas_call | solution.py:487
  29.4 0.8 %shard_map.111 = (bf16[128,384]{1,0:T(8,128)(2,1)}, bf16[128,256]{1,0:T(8,128)(2,1)}, bf16[128,256]{1,0:T(8,128)(2,1)}, f32[32,128]{1,0:T(8,128)}, f32[32,512]{1,0:T(8,128)}) custom-call(bf16[128,384]{1,0:T(8,128)(2,1)S(1)} %get-tuple-element.15.refs_0_, bf16[128,256]{1,0:T(8,128)(2,1)S(1)} %get-tuple-element.16.refs_1_, ...), custom_call_target="tpu_custom_call" | custom-call | tf_op jit(solution)/shard_map/pallas_call | solution.py:497

commit v3 on v2

--- a/solution.py
+++ b/solution.py
@@ -74,7 +74,7 @@
     return sorted(range(1, n), key=lambda d: -bin(d).count("1"))
 
 
-def kernel(
+def general_kernel(
     S, TP, H, GY, GX,
     q_in, lat_in, rot_in, w_in, log_in, out_in, go_in,
     qg_ref, kg_ref, vg_ref, rg_ref, wg_ref,
@@ -445,6 +445,361 @@
     lax.fori_loop(1, S, left, 0)
 
 
+def one_stage_kernel(
+    S, H, Z,
+    q_in, lat_in, rot_in, w_in, log_in, out_in, go_in,
+    qg_ref, kg_ref, vg_ref, rg_ref, wg_ref,
+    q_ref, lat_ref, rot_ref, w_ref, log_ref, out_ref, go_ref, loads,
+    qs, pk, wq, kb, lb, rp, key_ref, value_ref, turned_ref, dqa, dqx, dqr, dka, dva,
+    kvo, kvh, ro, rr, rt, wgs, wgr, dqo, dqh,
+    s1q, r1q, s1k, r1k, s2q, r2q, s3l, r3l, s4l, r4l, s5d, r5d,
+    s6k, r6k, s6r, r6r, s6q, r6q, s7, r7, s8, r8,
+):
+    TP = 2
+    NH = TP * H
+    T = q_ref.shape[0]
+    me = lax.axis_index("sp")
+    c = lax.axis_index("tp")
+    zh, g = me // NH, lax.rem(me, NH)
+    k, p = g // H, lax.rem(g, H)
+    straight = 1 - (c - k) * (c - k)
+    scale = HEAD ** (-0.5)
+    log2e = math.log2(math.e)
+    far = distances(H)
+    order = [0] + far
+    quarter = T * ROPE // LANES
+    wide = H * T
+
+    barrier = pltpu.get_barrier_semaphore()
+
+    def chip(z, kk, pp):
+        return lax.rem(zh + z, Z) * NH + kk * H + pp
+
+    def device(sp, tp):
+        return {"sp": sp, "tp": tp}
+
+    def copy(src, dst, ssem, rsem, where):
+        return pltpu.make_async_remote_copy(
+            src_ref=src, dst_ref=dst, send_sem=ssem, recv_sem=rsem,
+            device_id=where, device_id_type=MESH,
+        )
+
+    def greet(where):
+        pl.semaphore_signal(barrier, inc=1, device_id=where, device_id_type=MESH)
+
+    sibling = device(me, 1 - c)
+
+    pairs = (
+        (q_in, q_ref), (go_in, go_ref), (out_in, out_ref), (log_in, log_ref),
+        (lat_in, lat_ref), (w_in, w_ref), (rot_in, rot_ref),
+    )
+    fetch = [pltpu.make_async_copy(u, v, loads.at[i]) for i, (u, v) in enumerate(pairs)]
+    for f in fetch:
+        f.start()
+
+    def at(d):
+        return partner(H, p, d, 1)
+
+    def unless_self(z, d, body):
+        if z == 0 and d == 0:
+            pl.when(straight == 0)(body)
+        else:
+            body()
+
+    for z in range(Z - 1, -1, -1):
+        for d in order:
+            unless_self(z, d, lambda: greet(device(chip(z, c, at(d)), k)))
+    for d in far:
+        greet(device(chip(0, k, at(d)), c))
+    greet(sibling)
+
+    for f in fetch[:4]:
+        f.wait()
+    prod = out_ref[...].astype(F32) * go_ref[...].astype(F32)
+    high = prod.astype(BF16)
+    rest = (prod - high.astype(F32)).astype(BF16)
+    head_of = lax.broadcasted_iota(jnp.int32, (8 * -(-H // 8), H * VDIM), 1) // VDIM
+    picks = (head_of == lax.broadcasted_iota(jnp.int32, head_of.shape, 0)).astype(F32).astype(BF16)
+    deltas = dot(picks, high, ((1,), (1,))) + dot(picks, rest, ((1,), (1,)))
+    logs = log_ref[...] * log2e
+    for j in range(H):
+        start = HEAD * j
+        qs[j, :T, :] = jnp.concatenate(
+            [q_ref[:, start : start + NOPE], go_ref[:, VDIM * j : VDIM * (j + 1)]], axis=1)
+        turned = q_ref[:, start + NOPE : start + HEAD]
+        qs[j, T : T + quarter, :] = jnp.concatenate(
+            [turned[quarter * i : quarter * (i + 1)] for i in range(LANES // ROPE)], axis=1)
+        terms = three_terms(logs[j : j + 1]) + three_terms(deltas[j : j + 1])
+        qs[j, T + quarter :, :] = jnp.concatenate(
+            [t.astype(F32) for t in terms] + [jnp.zeros((STATS - 6, T), F32)], axis=0).astype(BF16)
+
+    @pl.when(straight == 1)
+    def _():
+        wq[zh, c, p] = qs[p]
+
+    pl.semaphore_wait(barrier, Z * H - straight + H - 1 + 1)
+
+    def send_q(z, d):
+        return copy(qs.at[at(d)], wq.at[zh, k, p], s1q.at[z, d], r1q.at[z, d], device(chip(z, c, at(d)), k))
+
+    def take_q(z, d):
+        place = wq.at[lax.rem(zh + z, Z), c, at(d)]
+        return copy(place, place, s1q.at[z, d], r1q.at[(Z - z) % Z, d], sibling)
+
+    def send_k(d):
+        return copy(pk.at[at(d)], kb.at[p], s1k.at[d], r1k.at[d], device(chip(0, c, at(d)), k))
+
+    def take_k(d):
+        place = kb.at[at(d)]
+        return copy(place, place, s1k.at[d], r1k.at[d], sibling)
+
+    def pass_q(z, d):
+        place = wq.at[lax.rem(zh + z, Z), c, at(d)]
+        return copy(place, place, s2q.at[z, d], r2q.at[z, d], sibling)
+
+    def passed_q(z, d):
+        place = wq.at[lax.rem(zh + z, Z), 1 - c, at(d)]
+        return copy(place, place, s2q.at[z, d], r2q.at[z, d], sibling)
+
+    by_hops = far + [0]
+    for d in by_hops:
+        unless_self(0, d, lambda: send_q(0, d).start())
+    for f in fetch[4:]:
+        f.wait()
+    joined = dot(lat_ref[...], w_ref[...], ((1,), (0,))).astype(BF16)
+    for j in range(H):
+        pk[j, :T, :] = joined[:, LANES * j : LANES * (j + 1)]
+        pk[j, T:, :] = rot_ref[...]
+    for d in by_hops:
+        unless_self(0, d, lambda: send_k(d).start())
+    for z in range(1, Z):
+        for d in by_hops:
+            send_q(z, d).start()
+
+    @pl.when(straight == 1)
+    def _():
+        kb[p] = pk[p]
+        lb[p] = lat_ref[...]
+
+    def cross_l():
+        return copy(lat_ref, lb.at[p], s3l, r3l, device(chip(0, c, p), k))
+
+    pl.when(straight == 0)(lambda: cross_l().start())
+
+    def take_all(z):
+        for d in order:
+            unless_self(z, d, lambda: take_q(z, d).wait_recv())
+            pass_q(z, d).start()
+
+    take_all(0)
+    for d in order:
+        unless_self(0, d, lambda: take_k(d).wait_recv())
+
+    lane = lax.broadcasted_iota(jnp.int32, (T, LANES), 1)
+    for j in range(H):
+        kv = kb[j, :T, :]
+        rot = kb[j, T:, :]
+        part = jnp.where(lane < NOPE, kv, jnp.zeros_like(kv))
+        column = rot.astype(F32).T.astype(BF16)
+        key_ref[T * j : T * (j + 1), :LANES] = part
+        key_ref[T * j : T * (j + 1), LANES:] = jnp.concatenate(
+            [column, jnp.zeros((T, LANES - ROPE), BF16)], axis=1)
+        value_ref[T * j : T * (j + 1), :] = kv - part
+        turned_ref[:NOPE, T * j : T * (j + 1)] = kv.astype(F32).T.astype(BF16)[:NOPE]
+        turned_ref[NOPE:, T * j : T * (j + 1)] = rot
+
+    def attend(z, kk):
+        zs = lax.rem(zh + z, Z)
+        ks = lax.rem(c + kk, TP)
+        for j in range(H):
+            packed = wq[zs, ks, j, T : T + quarter, :]
+            for i in range(LANES // ROPE):
+                turn = packed if i == 0 else jnp.concatenate(
+                    [packed[:, ROPE * i :], packed[:, : ROPE * i]], axis=1)
+                rp[T * j + quarter * i : T * j + quarter * (i + 1), :] = turn
+        row = wq[zs, ks, :, :T, :].reshape(wide, LANES)
+        both = jnp.concatenate([row, rp[...]], axis=1)
+        stats = [wq[zs, ks, j, T + quarter :, :].astype(F32) for j in range(H)]
+        log = jnp.concatenate([t[0:1] + t[1:2] + t[2:3] for t in stats], axis=1)
+        delta = jnp.concatenate([t[3:4] + t[4:5] + t[5:6] for t in stats], axis=1)
+        s = dot(key_ref[...], both, ((1,), (1,)))
+        dp = dot(value_ref[...], row, ((1,), (1,)))
+        prob = jnp.exp2(s * (scale * log2e) - log)
+        ds = (prob * (dp - delta)).astype(BF16)
+        dq = dot(turned_ref[...], ds, ((1,), (0,)))
+        dk = dot(ds, both, ((1,), (0,)))
+        dv = dot(prob.astype(BF16), row, ((1,), (0,)))
+        return dq, dk, dv
+
+    def gather(z, kk):
+        dq, dk, dv = attend(z, kk)
+        if kk == 0:
+            dqa[z] = dq
+        else:
+            dqx[z] = dq
+            swap_d(z).start()
+        if z == 0 and kk == 0:
+            dka[...], dva[...] = dk, dv
+        else:
+            dka[...] += dk
+            dva[...] += dv
+
+    def swap_d(z):
+        return copy(dqx.at[z], dqr.at[z], s5d.at[z], r5d.at[z], sibling)
+
+    def home_q(z, d):
+        return copy(dqo.at[z, at(d)], dqh.at[zh, p], s6q.at[z, d], r6q.at[z, d],
+                    device(chip(z, c, at(d)), k))
+
+    def home_took_q(z, d):
+        place = dqh.at[lax.rem(zh + z, Z), at(d)]
+        return copy(place, place, s6q.at[z, d], r6q.at[(Z - z) % Z, d], sibling)
+
+    def finish_q(z):
+        swap_d(z).wait_recv()
+        total = ((dqa[z] + dqr[z]) * scale).astype(BF16)
+        for j in range(H):
+            dqo[z, j] = total[:, T * j : T * (j + 1)]
+        for d in by_hops:
+            unless_self(z, d, lambda: home_q(z, d).start())
+        if z == 0:
+            @pl.when(straight == 1)
+            def _():
+                dqh[zh, p] = dqo[0, p]
+
+    def plane_l(d):
+        return copy(lb.at[p], lb.at[p], s4l.at[d - 1], r4l.at[d - 1], device(chip(0, k, at(d)), c))
+
+    def take_l(d):
+        place = lb.at[at(d)]
+        return copy(place, place, s4l.at[d - 1], r4l.at[d - 1], sibling)
+
+    gather(0, 0)
+    pl.when(straight == 0)(lambda: cross_l().wait_recv())
+    for d in far:
+        plane_l(d).start()
+    for d in order:
+        passed_q(0, d).wait_recv()
+    gather(0, 1)
+    for z in range(1, Z):
+        take_all(z)
+        if z == 1:
+            finish_q(0)
+        gather(z, 0)
+        for d in order:
+            passed_q(z, d).wait_recv()
+        gather(z, 1)
+    if Z == 1:
+        finish_q(0)
+
+    dk, dv = dka[...] * scale, dva[...]
+    lane = lax.broadcasted_iota(jnp.int32, dv.shape, 1)
+    kv = jnp.where(lane < NOPE, dk[:, :LANES], dv).astype(BF16)
+    rot = dk[:, LANES:].T[:ROPE]
+    for j in range(H):
+        kvo[j] = kv[T * j : T * (j + 1)]
+        ro[j] = rot[:, T * j : T * (j + 1)]
+
+    def home_k(d):
+        return copy(kvo.at[at(d)], kvh.at[p], s6k.at[d], r6k.at[d], device(chip(0, c, at(d)), k))
+
+    def home_r(d):
+        return copy(ro.at[at(d)], rr.at[p], s6r.at[d], r6r.at[d], device(chip(0, c, at(d)), k))
+
+    def home_took_k(d):
+        place = kvh.at[at(d)]
+        return copy(place, place, s6k.at[d], r6k.at[d], sibling)
+
+    def home_took_r(d):
+        place = rr.at[at(d)]
+        return copy(place, place, s6r.at[d], r6r.at[d], sibling)
+
+    for d in by_hops:
+        unless_self(0, d, lambda: home_k(d).start())
+
+    for d in far:
+        take_l(d).wait_recv()
+    rows = wgs.shape[1]
+    total = dot(lb[...].reshape(wide, lb.shape[2]), kv, ((0,), (0,)))
+    wgs[...] = total.reshape(S, rows, LANES).astype(WG_PART)
+    spread = [(z, kk, d) for z in range(Z - 1, -1, -1) for kk in (1, 0) for d in by_hops]
+
+    def at_k(kk):
+        return lax.rem(k + kk, TP)
+
+    def share(z, kk, d):
+        to = chip(z, at_k(kk), at(d))
+        return copy(wgs.at[to], wgr.at[zh, c, p], s7.at[z, kk, d], r7.at[z, c, d], device(to, k))
+
+    @pl.when(straight == 1)
+    def _():
+        kvh[p] = kvo[p]
+        rr[p] = ro[p]
+        wgr[zh, c, p] = wgs[me]
+
+    def unless_own(z, kk, d, body):
+        if kk == 0:
+            unless_self(z, d, body)
+        else:
+            body()
+
+    def take_share(z, kk, d):
+        core = lax.rem(c + kk, TP)
+        place = wgr.at[lax.rem(zh + z, Z), core, at(d)]
+        return copy(place, place, s7.at[z, kk, d], r7.at[(Z - z) % Z, core, d], sibling)
+
+    for z, kk, d in spread:
+        unless_own(z, kk, d, lambda: share(z, kk, d).start())
+    for z in range(1, Z):
+        finish_q(z)
+    for d in by_hops:
+        unless_self(0, d, lambda: home_r(d).start())
+
+    for d in order:
+        unless_self(0, d, lambda: home_took_k(d).wait_recv())
+    for j in range(H):
+        kg_ref[:, NOPE * j : NOPE * (j + 1)] = kvh[j, :, :NOPE]
+        vg_ref[:, VDIM * j : VDIM * (j + 1)] = kvh[j, :, NOPE:]
+    for d in order:
+        unless_self(0, d, lambda: home_took_r(d).wait_recv())
+    rt[c] = add_all([rr[j] for j in range(H)])
+
+    def swap():
+        return copy(rt.at[c], rt.at[c], s8, r8, sibling)
+
+    swap().start()
+    for z in range(Z):
+        for d in order:
+            unless_self(z, d, lambda: home_took_q(z, d).wait_recv())
+    summed = add_all([dqh[z].reshape(H * HEAD, T).astype(F32) for z in range(Z)])
+    qg_ref[...] = summed.T.astype(BF16)
+    pltpu.make_async_remote_copy(
+        src_ref=rt.at[1 - c], dst_ref=rt.at[1 - c], send_sem=s8, recv_sem=r8,
+        device_id=sibling, device_id_type=MESH).wait_recv()
+    rg_ref[...] = add_all([rt[i] for i in range(TP)])
+    for z, kk, d in spread:
+        unless_own(z, kk, d, lambda: take_share(z, kk, d).wait_recv())
+    for j in range(H):
+        wg_ref[:, LANES * j : LANES * (j + 1)] = add_all(
+            [wgr[z, i, j].astype(F32) for z in range(Z) for i in range(TP)])
+
+    for z in range(Z):
+        for d in order:
+            unless_self(z, d, lambda: send_q(z, d).wait_send())
+            unless_self(z, d, lambda: home_q(z, d).wait_send())
+            pass_q(z, d).wait_send()
+        swap_d(z).wait_send()
+    for d in order:
+        for what in (send_k, home_k, home_r):
+            unless_self(0, d, lambda: what(d).wait_send())
+    for d in far:
+        plane_l(d).wait_send()
+    pl.when(straight == 0)(lambda: cross_l().wait_send())
+    for z, kk, d in spread:
+        unless_own(z, kk, d, lambda: share(z, kk, d).wait_send())
+    swap().wait_send()
+
+
 def put_out(*refs):
     copies = [pltpu.make_async_copy(refs[i], refs[5 + i], refs[10].at[i]) for i in range(5)]
     for c in copies:
@@ -453,20 +808,26 @@
         c.wait()
 
 
-def per_device(S, TP, queries, latents, rot_key, kv_weight, log_sums, outputs, out_grad):
-    T, rank = latents.shape
-    H = log_sums.shape[1]
+def dma(*n):
+    return pltpu.SemaphoreType.DMA(tuple(max(k, 1) for k in n))
+
+
+def pairs(*n):
+    return [dma(*n), dma(*n)]
+
+
+def vm(shape, kind):
+    return pltpu.VMEM(tuple(max(k, 1) for k in shape), kind)
+
+
+def general_plan(S, TP, H, T, rank, arrays):
     G = S // H
     GX = max(d for d in range(1, math.isqrt(G) + 1) if G % d == 0)
     GY = G // GX
     rows = rank // S
     wide = H * T
-    dma = lambda *n: pltpu.SemaphoreType.DMA(tuple(max(k, 1) for k in n))
-    pairs = lambda *n: [dma(*n), dma(*n)]
-    vm = lambda shape, kind: pltpu.VMEM(tuple(max(k, 1) for k in shape), kind)
     unit = T + T * ROPE // LANES + STATS
-    arrays = (queries, latents, rot_key.T, kv_weight, log_sums.T, outputs, out_grad)
-    scratch = [
+    return functools.partial(general_kernel, S, TP, H, GY, GX), [
         *[vm(u.shape, u.dtype) for u in arrays], dma(len(arrays)),
         vm((H, unit, LANES), BF16), vm((H, T + ROPE, LANES), BF16),
         vm((GY, H, unit, LANES), BF16), vm((GX, H, T + ROPE, LANES), BF16), vm((H, TP, T // TP, rank), BF16),
@@ -479,13 +840,42 @@
         *pairs(GY - 1), *pairs(GX - 1, H),
         *pairs(H - 1), *pairs(H - 1), *pairs(H - 1), *pairs(S - 1), *pairs(TP - 1), *pairs(H - 1, TP - 1),
     ]
+
+
+def one_stage_plan(S, H, T, rank, arrays):
+    Z = S // (2 * H)
+    rows = rank // S
+    wide = H * T
+    unit = T + T * ROPE // LANES + STATS
+    return functools.partial(one_stage_kernel, S, H, Z), [
+        *[vm(u.shape, u.dtype) for u in arrays], dma(len(arrays)),
+        vm((H, unit, LANES), BF16), vm((H, T + ROPE, LANES), BF16),
+        vm((Z, 2, H, unit, LANES), BF16), vm((H, T + ROPE, LANES), BF16), vm((H, T, rank), BF16),
+        vm((wide, LANES), BF16), vm((wide, 2 * LANES), BF16), vm((wide, LANES), BF16), vm((HEAD, wide), BF16),
+        *[vm((Z, HEAD, wide), F32)] * 3, vm((wide, 2 * LANES), F32), vm((wide, LANES), F32),
+        *[vm((H, T, LANES), BF16)] * 2, *[vm((H, ROPE, T), F32)] * 2, vm((2, ROPE, T), F32),
+        vm((S, rows, LANES), WG_PART), vm((Z, 2, H, rows, LANES), WG_PART), *[vm((Z, H, HEAD, T), BF16)] * 2,
+        *pairs(Z, H), *pairs(H), *pairs(Z, H), pltpu.SemaphoreType.DMA, pltpu.SemaphoreType.DMA, *pairs(H - 1),
+        *pairs(Z), *pairs(H), *pairs(H), *pairs(Z, H), *pairs(Z, 2, H), pltpu.SemaphoreType.DMA, pltpu.SemaphoreType.DMA,
+    ]
+
+
+def per_device(S, TP, queries, latents, rot_key, kv_weight, log_sums, outputs, out_grad):
+    T, rank = latents.shape
+    H = log_sums.shape[1]
+    rows = rank // S
+    arrays = (queries, latents, rot_key.T, kv_weight, log_sums.T, outputs, out_grad)
+    if TP == 2 and H > 1 and power_of_two(H) and S % (TP * H) == 0:
+        body, scratch = one_stage_plan(S, H, T, rank, arrays)
+    else:
+        body, scratch = general_plan(S, TP, H, T, rank, arrays)
     shapes = [
         ((T, H * HEAD), BF16), ((T, H * NOPE), BF16), ((T, H * VDIM), BF16),
         ((ROPE, T), F32), ((rows, H * LANES), F32),
     ]
     held = sum(u[0] * -(-u[1] // LANES) * LANES * jnp.dtype(t).itemsize for u, t in shapes)
     results = pl.pallas_call(
-        functools.partial(kernel, S, TP, H, GY, GX),
+        body,
         out_shape=[pltpu.VMEM(*u) for u in shapes],
         in_specs=[pl.BlockSpec(memory_space=pltpu.HBM)] * 7,
         out_specs=[pl.BlockSpec(memory_space=pltpu.VMEM)] * 5,

time: 30.3 us -> 35.1 us (1.16)
  Pallas kernels: 29.5 us -> 34.3 us
    pallas_call x1, Pallas kernels: 28.7 us -> 33.5 us  [per_device(): pl.pallas_call(body, out_shape=[pltpu.VMEM(*u) for u in shapes], in_specs...]
where the time goes in v3:
time: 35.1 us; the launch traced here: 34.9 us
  Pallas kernels  34.3 us (98%)
  between operations  0.64 us (2%)
    pallas_call x1, Pallas kernels, per_device(): pl.pallas_call(body, out_shape=[pltpu.VMEM(*u) for u in shapes], in_specs...  33.5 us
    pallas_call x1, Pallas kernels, per_device(): pl.pallas_call(put_out, out_shape=[jax.ShapeDtypeStruct(*u) for u in shap...  0.76 us

profile of v3, /device:TPU:0, one launch (start us, length us, event | category | flops | bytes accessed | tf_op | source)
XLA Modules:
  0.0 34.9 jit_solution(9058902945306561869)
XLA Ops:
  0.6 33.5 %shard_map.110 = (bf16[128,384]{1,0:T(8,128)(2,1)S(1)}, bf16[128,256]{1,0:T(8,128)(2,1)S(1)}, bf16[128,256]{1,0:T(8,128)(2,1)S(1)}, f32[32,128]{1,0:T(8,128)S(1)}, f32[32,512]{1,0:T(8,128)S(1)}) custom-call(bf16[128,384]{1,0:T(8,128)(2,1)} %q_in.1, bf16[128,512]{1,0:T(8,128)(2,1)} %lat_in.1, bf16[32,128]{1,0:T(8,128)(2,1)} %bitcast.3, ...), custom_call_target="tpu_custom_call" | custom-call | tf_op jit(solution)/shard_map/pallas_call | solution.py:877
  34.2 0.8 %shard_map.111 = (bf16[128,384]{1,0:T(8,128)(2,1)}, bf16[128,256]{1,0:T(8,128)(2,1)}, bf16[128,256]{1,0:T(8,128)(2,1)}, f32[32,128]{1,0:T(8,128)}, f32[32,512]{1,0:T(8,128)}) custom-call(bf16[128,384]{1,0:T(8,128)(2,1)S(1)} %get-tuple-element.15.refs_0_, bf16[128,256]{1,0:T(8,128)(2,1)S(1)} %get-tuple-element.16.refs_1_, ...), custom_call_target="tpu_custom_call" | custom-call | tf_op jit(solution)/shard_map/pallas_call | solution.py:887

commit v4 on v2

--- a/solution.py
+++ b/solution.py
@@ -79,10 +79,11 @@
     q_in, lat_in, rot_in, w_in, log_in, out_in, go_in,
     qg_ref, kg_ref, vg_ref, rg_ref, wg_ref,
     q_ref, lat_ref, rot_ref, w_ref, log_ref, out_ref, go_ref, loads,
-    qs, pk, wq, kb, lb, rp, dqa, dqs, dqr, kvs, kvr, dka, dva,
+    qs, pk, wq, kb, rk, lb, rp, key_ref, value_ref, turned_ref, dqa, dqs, dqr, kvs, kvr, rps, rpr, dka, dva,
     kvo, kvh, ro, rr, rt, wgs, wgr, dqo, dqh,
     s1q, r1q, s1k, r1k, s1l, r1l, s2q, r2q, s2k, r2k, s3q, r3q, s3k, r3k,
     s4q, r4q, s4k, r4k, s4r, r4r, s5, r5, s6, r6, s8, r8,
+    s9a, r9a, s9x, r9x, s9t, r9t, s9b, r9b,
 ):
     G = GY * GX
     T = q_ref.shape[0]
@@ -167,6 +168,30 @@
         to = partner(H, a, d, 1)
         return copy(pk.at[to], kb.at[x, a], s1k.at[d - 1], r1k.at[d - 1], at_a(to))
 
+    def first_r(d):
+        return copy(rot_ref, rk.at[x, a], s9a.at[d - 1], r9a.at[d - 1], at_a(partner(H, a, d, 1)))
+
+    def relay_r(d, e):
+        src = rk.at[x, partner(H, a, d, -1)]
+        return copy(src, src, s9x.at[e - 1, d], r9x.at[e - 1, d], at_x(e))
+
+    def over_r(d, e):
+        src = rk.at[lax.rem(x + e, GX), partner(H, a, d, -1)]
+        return pltpu.make_async_remote_copy(
+            src_ref=src, dst_ref=src, send_sem=s9t.at[e, d], recv_sem=r9t.at[e, d],
+            device_id={"tp": tpi + 1 - 2 * lax.rem(tpi, 2)}, device_id_type=MESH,
+        )
+
+    def leading(body):
+        if TP % 2:
+            body()
+        else:
+            pl.when(lax.rem(tpi, 2) == 1)(body)
+
+    def hand_over(d, e):
+        if TP % 2 == 0:
+            over_r(d, e).start()
+
     def relay_q(d, e):
         src = wq.at[y, partner(H, a, d, -1)]
         return copy(src, src, s2q.at[e - 1, d], r2q.at[e - 1, d], at_y(e))
@@ -182,12 +207,20 @@
         f.wait()
     joined = dot(lat_ref[...], w_ref[...], ((1,), (0,))).astype(BF16)
     for j in range(H):
-        pk[j, :T, :] = joined[:, LANES * j : LANES * (j + 1)]
-        pk[j, T:, :] = rot_ref[...]
+        pk[j] = joined[:, LANES * j : LANES * (j + 1)]
     kb[x, a] = pk[a]
+    rk[x, a] = rot_ref[...]
     for d in far:
         first_k(d).start()
     repeat(1, GX, lambda e: relay_k(0, e).start())
+
+    @leading
+    def _():
+        for d in far:
+            first_r(d).start()
+        for e in range(1, GX):
+            relay_r(0, e).start()
+
     lb[a] = lat_ref[...].reshape(lb.shape[1:])
     for d in far:
         first_q(d).wait_recv()
@@ -195,6 +228,14 @@
     for d in far:
         first_k(d).wait_recv()
         repeat(1, GX, lambda e: relay_k(d, e).start())
+
+    @leading
+    def _():
+        for d in far:
+            first_r(d).wait_recv()
+            for e in range(1, GX):
+                relay_r(d, e).start()
+            hand_over(d, 0)
 
     slab = T // TP
     mine = lat_ref.at[pl.ds(pl.multiple_of(tpi * slab, slab), slab)]
@@ -206,45 +247,59 @@
         piece = lb.at[partner(H, a, d, -1), tpi]
         return copy_tp(piece, piece, s8.at[d - 1, i - 1], r8.at[d - 1, i - 1], i)
 
-    for d in far:
-        first_l(d).start()
-
-    def keys_of(e, units):
+    wide = H * T
+    order = [0] + far
+    chunks = 2 if H % 2 == 0 else H
+    chunk = H // chunks
+    some = chunk * T
+
+    def unit_of(n, c):
+        return partner(H, a, order[n * chunk + c], -1)
+
+    def part_of(n):
+        return order[n * chunk : (n + 1) * chunk]
+
+    def prepare_keys(e, n):
         where = lax.rem(x + e, GX)
-        tall, wide, turned = [], [], []
-        for u in units:
-            kv = kb[where, u, :T, :]
-            rot = kb[where, u, T:, :]
-            lane = lax.broadcasted_iota(jnp.int32, (T, LANES), 1)
+        lane = lax.broadcasted_iota(jnp.int32, (T, LANES), 1)
+        for c in range(chunk):
+            rows = slice(T * c, T * (c + 1))
+            kv = kb[where, unit_of(n, c)]
+            rot = rk[where, unit_of(n, c)]
             part = jnp.where(lane < NOPE, kv, jnp.zeros_like(kv))
             column = rot.astype(F32).T.astype(BF16)
-            tall.append(jnp.concatenate([part, column, jnp.zeros((T, LANES - ROPE), BF16)], axis=1))
-            wide.append(kv - part)
-            turned.append(jnp.concatenate([kv.astype(F32).T.astype(BF16)[:NOPE], rot], axis=0))
-        return jnp.concatenate(tall, axis=0), jnp.concatenate(wide, axis=0), jnp.concatenate(turned, axis=1)
-
-    wide = H * T
-    order = [0] + far
-    chunk = 2 if H % 2 == 0 else 1
-    chunks = H // chunk
-
-    def prepare(f):
+            key_ref[e, n, rows, :LANES] = part
+            key_ref[e, n, rows, LANES:] = jnp.concatenate([column, jnp.zeros((T, LANES - ROPE), BF16)], axis=1)
+            value_ref[e, n, rows, :] = kv - part
+            turned_ref[e, n, :NOPE, rows] = kv.astype(F32).T.astype(BF16)[:NOPE]
+            turned_ref[e, n, NOPE:, rows] = rot
+
+    def prepare_queries(f, n):
         col = lax.rem(y + f, GY)
-        for j in range(H):
-            packed = wq[col, j, T : T + quarter, :]
-            for k in range(LANES // ROPE):
-                part = packed if k == 0 else jnp.concatenate(
-                    [packed[:, ROPE * k :], packed[:, : ROPE * k]], axis=1)
-                rp[f, T * j + quarter * k : T * j + quarter * (k + 1), :] = part
-
-    def attend(keys, f):
-        key, value, turned = keys
-        col = lax.rem(y + f, GY)
-        row = wq[col, :, :T, :].reshape(wide, LANES)
-        both = jnp.concatenate([row, rp[f]], axis=1)
-        stats = [wq[col, j, T + quarter :, :].astype(F32) for j in range(H)]
-        log = jnp.concatenate([t[0:1] + t[1:2] + t[2:3] for t in stats], axis=1)
-        delta = jnp.concatenate([t[3:4] + t[4:5] + t[5:6] for t in stats], axis=1)
+        for c in range(chunk):
+            packed = wq[col, unit_of(n, c), T : T + quarter, :]
+            for m in range(LANES // ROPE):
+                part = packed if m == 0 else jnp.concatenate(
+                    [packed[:, ROPE * m :], packed[:, : ROPE * m]], axis=1)
+                rp[f, n, T * c + quarter * m : T * c + quarter * (m + 1), :] = part
+
+    begun = set()
+
+    def attend(keys, queries):
+        key = jnp.concatenate([key_ref[e, n] for e, n in keys], axis=0)
+        value = jnp.concatenate([value_ref[e, n] for e, n in keys], axis=0)
+        turned = jnp.concatenate([turned_ref[e, n] for e, n in keys], axis=1)
+        rows, logs, deltas = [], [], []
+        for f, n in queries:
+            col = lax.rem(y + f, GY)
+            for c in range(chunk):
+                rows.append(wq[col, unit_of(n, c), :T, :])
+                t = wq[col, unit_of(n, c), T + quarter :, :].astype(F32)
+                logs.append(t[0:1] + t[1:2] + t[2:3])
+                deltas.append(t[3:4] + t[4:5] + t[5:6])
+        row = jnp.concatenate(rows, axis=0)
+        both = jnp.concatenate([row, jnp.concatenate([rp[f, n] for f, n in queries], axis=0)], axis=1)
+        log, delta = jnp.concatenate(logs, axis=1), jnp.concatenate(deltas, axis=1)
         s = dot(key, both, ((1,), (1,)))
         dp = dot(value, row, ((1,), (1,)))
         p = jnp.exp2(s * (scale * log2e) - log)
@@ -252,85 +307,133 @@
         dq = dot(turned, ds, ((1,), (0,)))
         dk = dot(ds, both, ((1,), (0,)))
         dv = dot(p.astype(BF16), row, ((1,), (0,)))
-        return dq, dk, dv
-
-    def unit_of(k, sign):
-        return partner(H, a, order[k], sign)
-
-    def span(n):
-        return pl.ds(wide // chunks * n, wide // chunks)
-
-    def keys_at(e, n):
-        return keys_of(e, [unit_of(n * chunk + c, -1) for c in range(chunk)])
-
-    def whole_keys(e):
-        return keys_of(e, [unit_of(k, -1) for k in range(H)])
-
-    def gather(e, n, dk, dv, first):
-        if first:
-            dka[e, span(n), :] = dk
-            dva[e, span(n), :] = dv
-        else:
-            dka[e, span(n), :] += dk
-            dva[e, span(n), :] += dv
-
-    def gather_all(e, dk, dv, first):
-        for n in range(chunks):
-            part = slice(wide // chunks * n, wide // chunks * (n + 1))
-            gather(e, n, dk[part], dv[part], first)
-
-    def totals(e, n):
-        dk, dv = dka[e, span(n), :], dva[e, span(n), :]
+        for i, (f, n) in enumerate(queries):
+            piece = dq[:, some * i : some * (i + 1)]
+            dqa[f, n] = dqa[f, n] + piece if ("q", f, n) in begun else piece
+            begun.add(("q", f, n))
+        for i, (e, n) in enumerate(keys):
+            span = slice(some * i, some * (i + 1))
+            if ("k", e, n) in begun:
+                dka[e, n] += dk[span]
+                dva[e, n] += dv[span]
+            else:
+                dka[e, n], dva[e, n] = dk[span], dv[span]
+            begun.add(("k", e, n))
+
+    def pair(e, n):
+        dk, dv = dka[e, n, :, :LANES], dva[e, n]
         lane = lax.broadcasted_iota(jnp.int32, dv.shape, 1)
-        dk = dk * scale
-        return jnp.where(lane < NOPE, dk[:, :LANES], dv), dk[:, LANES:].T[:ROPE]
+        return jnp.where(lane < NOPE, dk * scale, dv)
+
+    def turned_part(e):
+        return (jnp.concatenate([dka[e, n, :, LANES:] for n in range(chunks)], axis=0) * scale).T[:ROPE]
 
     def back_k(e, n):
         piece = pl.ds(n * chunk, chunk)
         return copy(kvs.at[e - 1, piece], kvr.at[e - 1, piece], s3k.at[e - 1, n], r3k.at[e - 1, n], at_x(e))
 
-    def back_q(f):
-        return copy(dqs.at[f - 1], dqr.at[f - 1], s3q.at[f - 1], r3q.at[f - 1], at_y(f))
+    def back_q(f, n):
+        return copy(dqs.at[f - 1, n], dqr.at[f - 1, n], s3q.at[f - 1, n], r3q.at[f - 1, n], at_y(f))
+
+    def back_r(e):
+        return copy(rps.at[e - 1], rpr.at[e - 1], s9b.at[e - 1], r9b.at[e - 1], at_x(e))
 
     def send_k(e, n):
-        kv, rot = totals(e, n)
+        kv = pair(e, n)
         for c in range(chunk):
-            kvs[e - 1, n * chunk + c, :T, :] = kv[T * c : T * (c + 1)].astype(KV_PART)
-            kvs[e - 1, n * chunk + c, T:, :] = rot[:, T * c : T * (c + 1)].astype(KV_PART)
+            kvs[e - 1, n * chunk + c] = kv[T * c : T * (c + 1)].astype(KV_PART)
         back_k(e, n).start()
 
-    prepare(0)
-    dq, dk, dv = attend(whole_keys(0), 0)
-    dqa[0] = dq
-    gather_all(0, dk, dv, True)
-    for e in range(1, GX):
-        for d in order:
+    def take_over(e, ds):
+        if TP % 2 == 0:
+            @pl.when(lax.rem(tpi, 2) == 0)
+            def _():
+                for d in ds:
+                    over_r(d, e).wait_recv()
+
+    def following(body):
+        if TP % 2:
+            body()
+        else:
+            pl.when(lax.rem(tpi, 2) == 0)(body)
+
+    take_over(0, far)
+    keys, queries = [], []
+    for n in range(chunks):
+        prepare_keys(0, n)
+        prepare_queries(0, n)
+        keys.append((0, n))
+        queries.append((0, n))
+    attend(keys, queries)
+    for d in far:
+        first_l(d).start()
+
+    def new_keys(e, n):
+        for d in part_of(n):
             relay_k(d, GX - e).wait_recv()
-        dq, dk, dv = attend(whole_keys(e), 0)
-        dqa[0] += dq
-        gather_all(e, dk, dv, True)
-    for f in range(1, GY):
-        for d in order:
+
+        @leading
+        def _():
+            for d in part_of(n):
+                relay_r(d, GX - e).wait_recv()
+                hand_over(d, e)
+
+        take_over(e, part_of(n))
+        prepare_keys(e, n)
+        attend([(e, n)], queries)
+        keys.append((e, n))
+
+    def latents_on():
+        for d in far:
+            first_l(d).wait_recv()
+            repeat(1, TP, lambda i: hand_on(d, i).start())
+
+    def close_queries(f, n):
+        dqs[f - 1, n] = dqa[f, n].astype(DQ_PART)
+        following(lambda: back_q(f, n).start())
+
+    def new_queries(f, n, last):
+        for d in part_of(n):
             relay_q(d, GY - f).wait_recv()
-        prepare(f)
+        prepare_queries(f, n)
+        if last:
+            others = [i for i in keys if i[0] > 0]
+            if others:
+                attend(others, [(f, n)])
+                for i in others:
+                    send_k(*i)
+            attend([i for i in keys if i[0] == 0], [(f, n)])
+        else:
+            attend(keys, [(f, n)])
+        queries.append((f, n))
+
+    more_keys = [(e, n) for e in range(1, GX) for n in range(chunks)]
+    more_queries = [(f, n) for f in range(1, GY) for n in range(chunks)]
+    lat_due = True
+    while more_keys or more_queries:
+        if more_keys:
+            new_keys(*more_keys.pop(0))
+            if not more_keys:
+                for i in queries:
+                    if i[0] > 0:
+                        close_queries(*i)
+        if lat_due and len(more_queries) <= 1:
+            latents_on()
+            lat_due = False
+        if more_queries:
+            i = more_queries.pop(0)
+            new_queries(*i, last=not more_keys and not more_queries)
+            if not more_keys:
+                close_queries(*i)
+    if lat_due:
+        latents_on()
+    if GY == 1:
         for e in range(1, GX):
             for n in range(chunks):
-                dq, dk, dv = attend(keys_at(e, n), f)
-                if e == 1 and n == 0:
-                    dqa[f] = dq
-                else:
-                    dqa[f] += dq
-                gather(e, n, dk, dv, False)
-                if f == GY - 1:
-                    send_k(e, n)
-        dq, dk, dv = attend(whole_keys(0), f)
-        dqs[f - 1] = (dqa[f] + dq if GX > 1 else dq).astype(DQ_PART)
-        back_q(f).start()
-        gather_all(0, dk, dv, False)
-
-    for d in far:
-        first_l(d).wait_recv()
-        repeat(1, TP, lambda i: hand_on(d, i).start())
+                send_k(e, n)
+    for e in range(1, GX):
+        rps[e - 1] = turned_part(e).astype(KV_PART)
+        back_r(e).start()
 
     def home_k(d):
         to = partner(H, a, d, -1)
@@ -346,23 +449,19 @@
     for n in range(chunks):
         for e in range(1, GX):
             back_k(e, n).wait_recv()
-        kv, rot = totals(0, n)
+        kv = pair(0, n)
         lats, finals = [], []
         for c in range(chunk):
             slot = n * chunk + c
-            u = unit_of(slot, -1)
-            part, turn = kv[T * c : T * (c + 1)], rot[:, T * c : T * (c + 1)]
+            part = kv[T * c : T * (c + 1)]
             for e in range(1, GX):
-                part = part + kvr[e - 1, slot, :T, :].astype(F32)
-                turn = turn + kvr[e - 1, slot, T:, :].astype(F32)
+                part = part + kvr[e - 1, slot].astype(F32)
             part = part.astype(BF16)
             kvo[slot] = part
-            ro[slot] = turn
-            lats.append(lb[u].reshape(T, lb.shape[3]))
+            lats.append(lb[unit_of(n, c)].reshape(T, lb.shape[3]))
             finals.append(part)
             if slot == 0:
                 kvh[a] = part
-                rr[a] = turn
             else:
                 home_k(order[slot]).start()
         grads.append(dot(jnp.concatenate(lats, axis=0), jnp.concatenate(finals, axis=0), ((0,), (0,))))
@@ -371,33 +470,47 @@
     wgs[...] = total.reshape(S, rows, LANES).astype(WG_PART)
     wgr[me] = wgs[me]
 
+    spread = distances(S)
+
     def share(i):
-        to = lax.rem(me + i, S)
+        to = partner(S, me, i, 1)
         return copy(wgs.at[to], wgr.at[me], s5.at[i - 1], r5.at[i - 1], to)
 
-    def spread(i, carry):
+    for i in spread:
         share(i).start()
-        return carry
-
-    lax.fori_loop(1, S, spread, 0)
+    @leading
+    def _():
+        if TP % 2 == 0:
+            for f in range(1, GY):
+                for n in range(chunks):
+                    back_q(f, n).start()
+
+    turned = turned_part(0)
+    for e in range(1, GX):
+        back_r(e).wait_recv()
+        turned = turned + rpr[e - 1].astype(F32)
+    for slot in range(H):
+        ro[slot] = turned[:, T * slot : T * (slot + 1)]
+    rr[a] = ro[0]
     for d in far:
         home_r(d).start()
 
-    mine_q = dqa[0]
-    for e in range(1, GY):
-        back_q(e).wait_recv()
-        mine_q = mine_q + dqr[e - 1].astype(F32)
-    mine_q = (mine_q * scale).astype(BF16)
-    for j in range(H):
-        dqo[j] = mine_q[:, T * j : T * (j + 1)]
-
     def home_q(d):
-        to = partner(H, a, d, 1)
-        return copy(dqo.at[to], dqh.at[a], s4q.at[d - 1], r4q.at[d - 1], at_a(to))
-
-    for d in far:
-        home_q(d).start()
-    dqh[a] = dqo[a]
+        to = partner(H, a, d, -1)
+        return copy(dqo.at[order.index(d)], dqh.at[a], s4q.at[d - 1], r4q.at[d - 1], at_a(to))
+
+    for n in range(chunks):
+        mine_q = dqa[0, n]
+        for f in range(1, GY):
+            back_q(f, n).wait_recv()
+            mine_q = mine_q + dqr[f - 1, n].astype(F32)
+        mine_q = (mine_q * scale).astype(BF16)
+        for c, d in enumerate(part_of(n)):
+            dqo[n * chunk + c] = mine_q[:, T * c : T * (c + 1)]
+            if d == 0:
+                dqh[a] = dqo[0]
+            else:
+                home_q(d).start()
 
     for d in far:
         home_k(d).wait_recv()
@@ -418,11 +531,8 @@
     repeat(1, TP, lambda i: swap(i).wait_recv())
     rg_ref[...] = add_all([rt[i] for i in range(TP)])
 
-    def arrive(i, carry):
+    for i in spread:
         share(i).wait_recv()
-        return carry
-
-    lax.fori_loop(1, S, arrive, 0)
     for j in range(H):
         wg_ref[:, LANES * j : LANES * (j + 1)] = add_all([wgr[i * H + j].astype(F32) for i in range(G)])
 
@@ -435,14 +545,29 @@
         repeat(1, GX, lambda e: relay_k(d, e).wait_send())
     for n in range(chunks):
         repeat(1, GX, lambda e: back_k(e, n).wait_send())
-    repeat(1, GY, lambda e: back_q(e).wait_send())
+    for f in range(1, GY):
+        for n in range(chunks):
+            back_q(f, n).wait_send()
     repeat(1, TP, lambda i: swap(i).wait_send())
-
-    def left(i, carry):
+    for i in spread:
         share(i).wait_send()
-        return carry
-
-    lax.fori_loop(1, S, left, 0)
+
+    @leading
+    def _():
+        for d in far:
+            first_r(d).wait_send()
+        for e in range(1, GX):
+            for d in order:
+                relay_r(d, e).wait_send()
+        if TP % 2 == 0:
+            for d in far:
+                over_r(d, 0).wait_send()
+            for e in range(1, GX):
+                for d in order:
+                    over_r(d, e).wait_send()
+
+    for e in range(1, GX):
+        back_r(e).wait_send()
 
 
 def put_out(*refs):
@@ -465,19 +590,23 @@
     pairs = lambda *n: [dma(*n), dma(*n)]
     vm = lambda shape, kind: pltpu.VMEM(tuple(max(k, 1) for k in shape), kind)
     unit = T + T * ROPE // LANES + STATS
+    chunks = 2 if H % 2 == 0 else H
+    some = wide // chunks
     arrays = (queries, latents, rot_key.T, kv_weight, log_sums.T, outputs, out_grad)
     scratch = [
         *[vm(u.shape, u.dtype) for u in arrays], dma(len(arrays)),
-        vm((H, unit, LANES), BF16), vm((H, T + ROPE, LANES), BF16),
-        vm((GY, H, unit, LANES), BF16), vm((GX, H, T + ROPE, LANES), BF16), vm((H, TP, T // TP, rank), BF16),
-        vm((GY, wide, LANES), BF16), vm((GY, HEAD, wide), F32),
-        *[vm((GY - 1, HEAD, wide), DQ_PART)] * 2, *[vm((GX - 1, H, T + ROPE, LANES), KV_PART)] * 2,
-        vm((GX, wide, 2 * LANES), F32), vm((GX, wide, LANES), F32),
+        vm((H, unit, LANES), BF16), vm((H, T, LANES), BF16),
+        vm((GY, H, unit, LANES), BF16), vm((GX, H, T, LANES), BF16), vm((GX, H, ROPE, T), BF16), vm((H, TP, T // TP, rank), BF16),
+        vm((GY, chunks, some, LANES), BF16), vm((GX, chunks, some, 2 * LANES), BF16),
+        vm((GX, chunks, some, LANES), BF16), vm((GX, chunks, HEAD, some), BF16), vm((GY, chunks, HEAD, some), F32),
+        *[vm((GY - 1, chunks, HEAD, some), DQ_PART)] * 2, *[vm((GX - 1, H, T, LANES), KV_PART)] * 2, *[vm((GX - 1, ROPE, wide), KV_PART)] * 2,
+        vm((GX, chunks, some, 2 * LANES), F32), vm((GX, chunks, some, LANES), F32),
         *[vm((H, T, LANES), BF16)] * 2, *[vm((H, ROPE, T), F32)] * 2, vm((TP, ROPE, T), F32),
         *[vm((S, rows, LANES), WG_PART)] * 2, *[vm((H, HEAD, T), BF16)] * 2,
         *pairs(H - 1), *pairs(H - 1), *pairs(H - 1), *pairs(GY - 1, H), *pairs(GX - 1, H),
-        *pairs(GY - 1), *pairs(GX - 1, H),
+        *pairs(GY - 1, chunks), *pairs(GX - 1, chunks),
         *pairs(H - 1), *pairs(H - 1), *pairs(H - 1), *pairs(S - 1), *pairs(TP - 1), *pairs(H - 1, TP - 1),
+        *pairs(H - 1), *pairs(GX - 1, H), *pairs(GX, H), *pairs(GX - 1),
     ]
     shapes = [
         ((T, H * HEAD), BF16), ((T, H * NOPE), BF16), ((T, H * VDIM), BF16),

time: 30.3 us -> 33.1 us (1.092)
  the two profiles are of different devices: /device:TPU:0 before, /device:TPU:1 now
where the time goes in v4:
time: 33.1 us; the launch traced here: 32.9 us
  Pallas kernels  32.3 us (98%)
  between operations  0.64 us (2%)
    pallas_call x1, Pallas kernels, per_device(): pl.pallas_call(functools.partial(kernel, S, TP, H, GY, GX), out_shape=[pl...  31.5 us
    pallas_call x1, Pallas kernels, per_device(): pl.pallas_call(put_out, out_shape=[jax.ShapeDtypeStruct(*u) for u in shap...  0.76 us

profile of v4, /device:TPU:1, one launch (start us, length us, event | category | flops | bytes accessed | tf_op | source)
XLA Modules:
  0.0 32.9 jit_solution(1034927122470698425)
XLA Ops:
  0.6 31.5 %shard_map.110 = (bf16[128,384]{1,0:T(8,128)(2,1)S(1)}, bf16[128,256]{1,0:T(8,128)(2,1)S(1)}, bf16[128,256]{1,0:T(8,128)(2,1)S(1)}, f32[32,128]{1,0:T(8,128)S(1)}, f32[32,512]{1,0:T(8,128)S(1)}) custom-call(bf16[128,384]{1,0:T(8,128)(2,1)} %q_in.1, bf16[128,512]{1,0:T(8,128)(2,1)} %lat_in.1, bf16[32,128]{1,0:T(8,128)(2,1)} %bitcast.3, ...), custom_call_target="tpu_custom_call" | custom-call | tf_op jit(solution)/shard_map/pallas_call | solution.py:616
  32.2 0.8 %shard_map.111 = (bf16[128,384]{1,0:T(8,128)(2,1)}, bf16[128,256]{1,0:T(8,128)(2,1)}, bf16[128,256]{1,0:T(8,128)(2,1)}, f32[32,128]{1,0:T(8,128)}, f32[32,512]{1,0:T(8,128)}) custom-call(bf16[128,384]{1,0:T(8,128)(2,1)S(1)} %get-tuple-element.15.refs_0_, bf16[128,256]{1,0:T(8,128)(2,1)S(1)} %get-tuple-element.16.refs_1_, ...), custom_call_target="tpu_custom_call" | custom-call | tf_op jit(solution)/shard_map/pallas_call | solution.py:626
